TPU v7x, 512 devices: a whole 4x4x16 slice. The times are simulated.
512 devices in a mesh: gr: 2 (over z_hi), sp: 32 (over z_lo, y), tp: 8 (over x, core).
Axes of the slice: x: 4, y: 4, z: 16 (z_hi: 2, z_lo: 8; z = z_hi * 8 + z_lo), core: 2. Of those that a mesh axis runs over, the one named last changes fastest.
Arguments:
- tokens: bfloat16 [8, 4096, 4096], P('gr', 'sp'), parts along dimension 0, may hold values from -6 to 6
- key_weight: bfloat16 [4096, 2048], P('sp', 'tp'), may hold values from -0.09375 to 0.09375
- value_weight: bfloat16 [4096, 2048], P('sp', 'tp'), may hold values from -0.09375 to 0.09375
- log_decay: float32 [32, 8, 4096], P('tp', 'gr', 'sp'), parts along dimension 1, may hold values from -1 to 0, as said below
- new_query: bfloat16 [8, 2048], P('gr', 'tp'), parts along dimension 0, may hold values from -6 to 6
- new_key: bfloat16 [8, 2048], P('gr', 'tp'), parts along dimension 0, may hold values from -24 to 24
- new_value: bfloat16 [8, 2048], P('gr', 'tp'), parts along dimension 0, may hold values from -6 to 6
- step_decay: float32 [32, 8], P('tp', 'gr'), parts along dimension 1, may hold values from -1.5 to -0.05
- norm_gain: float32 [2048], P('tp'), may hold values from 0.1 to 1.9
Outputs:
- state_cache: float32 [512, 32, 64], P('gr', 'tp'), parts along dimension 0
- first_read: bfloat16 [8, 2048], P('gr', 'tp'), parts along dimension 0
There are 2 independent parts, one for each index of `gr`. A program takes and returns all parts, laid end to end along the dimension named above; an argument that names none is the same for every part. Nothing has to cross between parts.
Inputs may be any that keep to these rules, and one draw needn't show every extreme that they name: `log_decay`: every entry is at most zero.
All inputs are finite; a program needn't handle non-finite values.
Results may differ from a plain program's by a relative error of at most 0.0053.
Values may be sent and summed in bfloat16 or wider, within the bound.
No kernel may reach another device: no remote copies, remote signals or barrier semaphores. Data moves between devices by JAX's collectives and lax.ppermute only.
A program may use at most 64 MiB of HBM per device.

v0:
```python
import functools

import jax
import jax.numpy as jnp
from jax import lax
from jax.experimental import pallas as pl
from jax.experimental.pallas import tpu as pltpu
from jax.sharding import PartitionSpec as P

HEAD_DIM = 64
Y = 4
PARTS = 3
EXTRA = 128
EXACT = lax.Precision.HIGHEST
F32, BF16 = (jnp.float32, jnp.bfloat16)


def moved_along_z(x, by):
    ring = lax.axis_size("gr") * lax.axis_size("sp") // Y
    pairs = [(z * Y + y, (z + by) % ring * Y + y) for z in range(ring) for y in range(Y)]
    return lax.ppermute(x, ("gr", "sp"), pairs)


def from_opposite_plane(x):
    ring = lax.axis_size("gr") * lax.axis_size("sp") // Y
    wide = lax.axis_size("tp")
    far = lax.axis_size("sp") // Y // 2
    pairs = []
    for z in range(ring):
        for y in range(Y):
            for t in range(wide):
                to = (z + (far if t % 2 else -far)) % ring
                pairs.append(((z * Y + y) * wide + t, (to * Y + y) * wide + t))
    return lax.ppermute(x, ("gr", "sp", "tp"), pairs)


def moved_along_y(x, by):
    planes = lax.axis_size("sp") // Y
    pairs = [(z * Y + y, z * Y + (y + by) % Y) for z in range(planes) for y in range(Y)]
    return lax.ppermute(x, "sp", pairs)


def exchanged_along_y(spread):
    groups = [[z * Y + y for y in range(Y)] for z in range(lax.axis_size("sp") // Y)]
    got = lax.all_to_all(spread, "sp", 0, 0, tiled=True, axis_index_groups=groups)
    return got.reshape(Y * got.shape[1], got.shape[2])


def projected(token_rows, own, spread):
    planes = lax.axis_size("sp") // Y
    far = planes // 2
    mine = lax.axis_index("sp").astype(jnp.uint32) // Y
    block = exchanged_along_y(spread)
    opposite = from_opposite_plane(own)
    depth = block.shape[0]
    row = lax.axis_index("sp").astype(jnp.uint32) % Y

    def part(weights, off, start=0):
        first = (mine + (off + planes)) % planes * depth + start
        cols = lax.dynamic_slice_in_dim(token_rows, first, weights.shape[0], 1)
        return jnp.dot(cols, weights, preferred_element_type=F32)

    def far_part(weights, by):
        return part(weights, far, (row + (Y - by)) % Y * own.shape[0])

    total = part(block, 0)
    up = down = block
    for hop in range(1, far):
        down = moved_along_z(down, -1)
        up = moved_along_z(up, 1)
        beside = moved_along_y(opposite, hop)
        if hop == 1:
            total += far_part(opposite, 0)
        total += far_part(beside, hop) + part(up, -hop) + part(down, hop)
    return total


def in_three(x):
    parts, rest = ([], x)
    for _ in range(PARTS):
        piece = lax.reduce_precision(rest, 8, 7)
        parts.append(piece.astype(jnp.bfloat16))
        rest = rest - piece
    return parts


def lanes_of(shape):
    return lax.broadcasted_iota(jnp.int32, shape, 1)


def rows_of(shape):
    return lax.broadcasted_iota(jnp.int32, shape, 0)


def spread_kernel(key_ref, value_ref, own_ref, spread_ref, sems):
    cols = key_ref.shape[1]
    copies = []
    for ref, cut in ((key_ref, pl.ds(0, cols)), (value_ref, pl.ds(cols, cols))):
        for to in (own_ref.at[:, cut], *(spread_ref.at[y, :, cut] for y in range(Y))):
            copies.append(pltpu.make_async_copy(ref, to, sems.at[len(copies)]))
    for copy in copies:
        copy.start()
    for copy in copies:
        copy.wait()


def share_kernel(seqs, sums_ref, cosine_ref, sine_ref, weight_ref, carried_ref, out_ref):
    cols = out_ref.shape[0]
    heads = cols // HEAD_DIM
    span = sums_ref.shape[0] // seqs
    half = HEAD_DIM // 2
    low = lanes_of((span, cols)) % HEAD_DIM < half
    spread = (rows_of((heads, cols)) == lanes_of((heads, cols)) // HEAD_DIM).astype(F32)
    blocks = [[] for _ in range(heads)]
    for seq in range(seqs):
        here = pl.ds(seq * span, span)
        keys = sums_ref[here, :cols].astype(BF16).astype(F32)
        values = sums_ref[here, cols:].astype(BF16)
        other = jnp.where(low, pltpu.roll(keys, cols - half, 1), pltpu.roll(keys, half, 1))
        turned = keys * cosine_ref[...] + other * sine_ref[...]
        faded = turned * jnp.dot(weight_ref[here, :], spread, precision=EXACT)
        high = faded.astype(BF16)
        rest = (faded - high.astype(F32)).astype(BF16)
        product = sum(
            lax.dot_general(
                values, part, (((0,), (0,)), ((), ())), preferred_element_type=F32
            )
            for part in (high, rest)
        )
        for head in range(heads):
            cut = slice(head * HEAD_DIM, (head + 1) * HEAD_DIM)
            blocks[head].append(product[cut, cut])
    for head in range(heads):
        cut = pl.ds(head * HEAD_DIM, HEAD_DIM)
        out_ref[cut, : seqs * HEAD_DIM] = jnp.concatenate(blocks[head], axis=1).astype(BF16)
    out_ref[:, seqs * HEAD_DIM :] = carried_ref[...]


def lines_kernel(
    place_ref, cosine_ref, sine_ref, query_ref, key_ref, value_ref, decay_ref, lines_ref, values_ref
):
    seqs, cols = query_ref.shape
    heads, lanes = (cols // HEAD_DIM, seqs * HEAD_DIM)
    rows, half = (values_ref.shape[0], HEAD_DIM // 2)
    mine = place_ref[0]
    head = mine * rows // HEAD_DIM
    low = lanes_of((seqs, cols)) % HEAD_DIM < half
    place = (cols, lanes)
    pick = (rows_of(place) // HEAD_DIM == head) & (
        rows_of(place) % HEAD_DIM == lanes_of(place) % HEAD_DIM
    )
    own = rows_of((seqs, lanes)) == lanes_of((seqs, lanes)) // HEAD_DIM

    def line(ref):
        u = ref[...].astype(F32)
        other = jnp.where(low, pltpu.roll(u, cols - half, 1), pltpu.roll(u, half, 1))
        turned = u * cosine_ref[...] + other * sine_ref[...]
        picked = jnp.dot(turned, pick.astype(F32), precision=EXACT)
        return jnp.sum(jnp.where(own, picked, 0.0), axis=0, keepdims=True)

    decay = jnp.dot(jnp.exp(decay_ref[...]), own.astype(F32), precision=EXACT)
    here = rows_of((heads, lanes)) == head
    lines_ref[0:1] = jnp.sum(jnp.where(here, decay, 0.0), axis=0, keepdims=True)
    lines_ref[1:2] = line(key_ref) * HEAD_DIM ** (-0.5)
    lines_ref[2:3] = line(query_ref)
    spot = lanes_of((rows, cols)) == mine * rows + rows_of((rows, cols))
    values = lax.dot_general(
        spot.astype(BF16), value_ref[...], (((1,), (1,)), ((), ())), preferred_element_type=F32
    )
    values_ref[...] = jnp.dot(values, own.astype(F32), precision=EXACT)


def owner_kernel(devices, seqs, got_ref, lines_ref, values_ref, out_ref):
    total, lanes = (got_ref.shape[0], seqs * HEAD_DIM)
    rows = total // devices
    later = (lanes_of((devices, total)) // rows > rows_of((devices, total))) & (
        lanes_of((devices, total)) % rows == 0
    )
    sums = jnp.dot(later.astype(BF16), got_ref[:, lanes:], preferred_element_type=F32)
    place = (EXTRA, lanes)
    wide = (rows_of(place) // PARTS == lanes_of(place) // HEAD_DIM).astype(F32)
    fade = jnp.exp(jnp.dot(sums, wide, precision=EXACT))
    shares = got_ref[:, :lanes].astype(F32)
    owned = shares[:rows] * fade[0:1]
    for device in range(1, devices):
        owned += shares[device * rows : (device + 1) * rows] * fade[device : device + 1]
    finished = lines_ref[0:1] * owned + lines_ref[1:2] * values_ref[...]
    place = (lanes, EXTRA)
    fold = rows_of(place) // HEAD_DIM == lanes_of(place) % seqs
    read = jnp.dot(finished * lines_ref[2:3], fold.astype(F32), precision=EXACT)
    piece = lanes_of(read.shape) // seqs
    rest, packed = (read, jnp.zeros_like(read))
    for part in range(PARTS):
        rounded = rest.astype(BF16).astype(F32)
        packed = jnp.where(piece == part, rounded, packed)
        rest = rest - rounded
    line = jnp.concatenate([finished, packed], axis=1)
    out_ref[...] = jnp.concatenate([line] * devices, axis=0).astype(BF16)


def read_kernel(seqs, got_ref, gain_ref, state_ref, read_ref):
    cols, lanes = (got_ref.shape[0], seqs * HEAD_DIM)
    state_ref[...] = got_ref[:, :lanes].astype(F32)
    place = (8, EXTRA)
    pick = (lanes_of(place) % seqs == rows_of(place)) & (lanes_of(place) < seqs * PARTS)
    raw = lax.dot_general(
        pick.astype(BF16), got_ref[:, lanes:], (((1,), (1,)), ((), ())), preferred_element_type=F32
    )
    place = (cols, cols)
    mean = (rows_of(place) // HEAD_DIM == lanes_of(place) // HEAD_DIM).astype(F32) / HEAD_DIM
    center = raw - jnp.dot(raw, mean, precision=EXACT)
    spread = jnp.dot(center * center, mean, precision=EXACT)
    normed = center * lax.rsqrt(spread + 1e-06) * gain_ref[...]
    read_ref[...] = normed[:seqs].astype(BF16)


def in_vmem(kernel, shapes, *operands):
    space = pl.BlockSpec(memory_space=pltpu.VMEM)
    many = isinstance(shapes, list)
    return pl.pallas_call(
        kernel,
        out_shape=shapes,
        in_specs=[space] * len(operands),
        out_specs=[space] * len(shapes) if many else space,
        compiler_params=pltpu.CompilerParams(vmem_limit_bytes=16 * 2**20),
    )(*operands)


def shards(
    tokens,
    key_weight,
    value_weight,
    log_decay,
    new_query,
    new_key,
    new_value,
    step_decay,
    norm_gain,
):
    seqs, span, width = tokens.shape
    heads = key_weight.shape[1] // HEAD_DIM
    cols = heads * HEAD_DIM
    lanes = seqs * HEAD_DIM
    half = HEAD_DIM // 2
    devices, mine = (lax.axis_size("sp"), lax.axis_index("sp"))
    rows = cols // devices

    positions = (mine * span + jnp.arange(span, dtype=jnp.int32)).astype(F32)
    inverse = 10000.0 ** (-jnp.arange(half, dtype=F32) * (2.0 / HEAD_DIM))
    angles = positions[:, None] * inverse
    cosine = jnp.tile(jnp.cos(angles), (1, 2 * heads)) * HEAD_DIM ** (-0.5)
    sine = jnp.sin(angles) * HEAD_DIM ** (-0.5)
    sine = jnp.tile(jnp.concatenate([-sine, sine], axis=1), (1, heads))
    totals = jnp.sum(log_decay, axis=-1)
    weight = jnp.exp(totals[:, :, None] - jnp.cumsum(log_decay, axis=-1))
    weight = jnp.transpose(weight, (1, 2, 0)).reshape(seqs * span, heads)
    carried = jnp.stack(in_three(totals), axis=-1).reshape(heads, 1, 1, seqs * PARTS)
    carried = jnp.broadcast_to(carried, (heads, devices // heads, 1, seqs * PARTS))
    carried = carried.reshape(devices, 1, seqs * PARTS)
    carried = jnp.pad(carried, ((0, 0), (0, rows - 1), (0, EXTRA - seqs * PARTS)))
    carried = carried.reshape(cols, EXTRA)

    last = float(span * devices) * inverse
    last_cosine = jnp.tile(jnp.cos(last), 2 * heads)[None]
    last_sine = jnp.sin(last)
    last_sine = jnp.tile(jnp.concatenate([-last_sine, last_sine]), heads)[None]
    ready = (cosine, sine, weight, carried, last_cosine, last_sine)
    cosine, sine, weight, carried, last_cosine, last_sine = lax.optimization_barrier(ready)

    depth = key_weight.shape[0]
    own, spread = pl.pallas_call(
        spread_kernel,
        out_shape=[
            jax.ShapeDtypeStruct((depth, 2 * cols), BF16),
            jax.ShapeDtypeStruct((Y, depth, 2 * cols), BF16),
        ],
        in_specs=[pl.BlockSpec(memory_space=pl.ANY)] * 2,
        out_specs=[pl.BlockSpec(memory_space=pltpu.VMEM)] * 2,
        scratch_shapes=[pltpu.SemaphoreType.DMA((2 * (Y + 1),))],
    )(key_weight, value_weight)
    sums = projected(tokens.reshape(seqs * span, width), own, spread)
    place = pl.BlockSpec(memory_space=pltpu.SMEM)
    space = pl.BlockSpec(memory_space=pltpu.VMEM)
    lines, value_rows = pl.pallas_call(
        lines_kernel,
        out_shape=[jax.ShapeDtypeStruct((3, lanes), F32), jax.ShapeDtypeStruct((rows, lanes), F32)],
        in_specs=[place] + [space] * 6,
        out_specs=[space] * 2,
        compiler_params=pltpu.CompilerParams(vmem_limit_bytes=2 * 2**20),
    )(
        mine[None],
        last_cosine,
        last_sine,
        new_query,
        new_key,
        new_value,
        step_decay,
    )
    whole = jax.ShapeDtypeStruct((cols, lanes + EXTRA), BF16)

    def exchanged(x):
        cut = x.reshape(devices, rows, lanes + EXTRA)
        return lax.all_to_all(cut, "sp", 0, 0, tiled=True).reshape(x.shape)

    sent = in_vmem(
        functools.partial(share_kernel, seqs), whole, sums, cosine, sine, weight, carried
    )
    finished = in_vmem(
        functools.partial(owner_kernel, devices, seqs), whole, exchanged(sent), lines, value_rows
    )
    state, first_read = in_vmem(
        functools.partial(read_kernel, seqs),
        [jax.ShapeDtypeStruct((cols, lanes), F32), jax.ShapeDtypeStruct((seqs, cols), BF16)],
        exchanged(finished),
        norm_gain.reshape(1, cols),
    )
    state_cache = jnp.transpose(state.reshape(heads, HEAD_DIM, lanes), (2, 0, 1))
    return (state_cache, first_read)


def solution(mesh):
    placed = (
        P("gr", "sp", None),
        P("sp", "tp"),
        P("sp", "tp"),
        P("tp", "gr", "sp"),
        P("gr", "tp"),
        P("gr", "tp"),
        P("gr", "tp"),
        P("tp", "gr"),
        P("tp"),
    )
    return jax.shard_map(
        shards,
        mesh=mesh,
        in_specs=placed,
        out_specs=(P("gr", "tp", None), P("gr", "tp")),
        check_vma=False,
    )
```

profile of v0, /device:TPU:2, one launch (start us, length us, event | category | flops | bytes accessed | tf_op | source)
XLA Modules:
  0.0 139.6 jit_solution(14755228998390954462)
XLA Ops:
  0.6 2.1 %shard_map.104 = (bf16[128,512]{1,0:T(8,128)(2,1)}, bf16[4,128,512]{2,1,0:T(8,128)(2,1)}) custom-call(bf16[128,256]{1,0:T(8,128)(2,1)} %key_ref.2, bf16[128,256]{1,0:T(8,128)(2,1)} %value_ref.2), custom_call_target="tpu_custom_call" | custom-call | tf_op jit(solution)/shard_map/pallas_call | solution.py:271
  2.7 4.5 %all-to-all-start = ((bf16[4,128,512]{2,1,0:T(8,128)(2,1)}), bf16[4,128,512]{2,1,0:T(8,128)(2,1)S(1)}, u32[]{:S(2)}, u32[]{:S(2)}) async-start(bf16[4,128,512]{2,1,0:T(8,128)(2,1)} %get-tuple-element.14), calls=%async_computation | async-start | bytes 1048576 | tf_op jit(solution)/shard_map/all_to_all | solution.py:45
  7.2 12.7 %collective-permute-start = (bf16[128,512]{1,0:T(8,128)(2,1)}, bf16[128,512]{1,0:T(8,128)(2,1)S(1)}, u32[]{:S(2)}, u32[]{:S(2)}) collective-permute-start(bf16[128,512]{1,0:T(8,128)(2,1)} %get-tuple-element.15), channel_id=1, source_target_pairs={{0,384},{1,129},{2,386},{3,131},{4,388},{5,133},{6,390},{7,135},{8... | collective-permute-start | bytes 393224 | tf_op jit(solution)/shard_map/ppermute | solution.py:34
  19.9 0.1 multiply_sine_fusion.1
  20.0 0.8 reduce_sum.11
  20.8 2.3 %reduce_window_sum.13 = f32[4,4,128]{2,1,0:T(4,128)S(1)} reduce-window(f32[4,4,128]{2,1,0:T(4,128)} %param.12, f32[]{:T(128)} %constant.121.clone.1), window={size=1x1x128 pad=0_0x0_0x127_0}, to_apply=%region_1.0 | reduce-window | flops 260096 | bytes 16388 | tf_op jit(solution)/shard_map/jit(cumsum)/reduce_window_sum | solution.py:255
  23.1 0.1 copy.14
  23.2 0.1 broadcast_in_dim.15
  23.3 0.1 fusion.25
  23.4 0.1 fusion.24
  23.5 0.1 multiply_cosine_fusion.1
  23.6 3.4 %collective-permute-done = bf16[128,512]{1,0:T(8,128)(2,1)S(1)} collective-permute-done((bf16[128,512]{1,0:T(8,128)(2,1)}, bf16[128,512]{1,0:T(8,128)(2,1)S(1)}, u32[]{:S(2)}, u32[]{:S(2)}) %collective-permute-start) | collective-permute-done | bytes 131104 | tf_op jit(solution)/shard_map/ppermute | solution.py:34
  26.9 5.1 %collective-permute-start.7 = (bf16[128,512]{1,0:T(8,128)(2,1)S(1)}, bf16[128,512]{1,0:T(8,128)(2,1)S(1)}, u32[]{:S(2)}, u32[]{:S(2)}) collective-permute-start(bf16[128,512]{1,0:T(8,128)(2,1)S(1)} %collective-permute-done), channel_id=1, source_target_pairs={{0,24},{8,0},{16,8},{24,16},{32,56},{40,32},{48,40},{56,48},{64,88... | collective-permute-start | bytes 393224 | tf_op jit(solution)/shard_map/ppermute | solution.py:40
  32.1 0.1 pad_maximum_fusion.2
  32.2 0.1 broadcast_in_dim_tile.7.sine_ref
  32.3 0.1 copy.13
  32.4 0.1 broadcast_in_dim_tile.6.cosine_ref
  32.6 0.1 copy.16.cosine_ref
  32.7 0.1 copy.17.sine_ref
  32.8 2.8 %collective-permute-start.4 = (bf16[128,512]{1,0:T(8,128)(2,1)S(1)}, bf16[128,512]{1,0:T(8,128)(2,1)S(1)}, u32[]{:S(2)}, u32[]{:S(2)}) collective-permute-start(bf16[128,512]{1,0:T(8,128)(2,1)S(1)} %collective-permute-done), channel_id=1, source_target_pairs={{0,16},{8,24},{16,0},{24,8},{32,48},{40,56},{48,32},{56,40},{64,80... | collective-permute-start | bytes 393224 | tf_op jit(solution)/shard_map/ppermute | solution.py:40
  35.5 2.8 %collective-permute-start.1 = (bf16[128,512]{1,0:T(8,128)(2,1)S(1)}, bf16[128,512]{1,0:T(8,128)(2,1)S(1)}, u32[]{:S(2)}, u32[]{:S(2)}) collective-permute-start(bf16[128,512]{1,0:T(8,128)(2,1)S(1)} %collective-permute-done), channel_id=1, source_target_pairs={{0,8},{8,16},{16,24},{24,0},{32,40},{40,48},{48,56},{56,32},{64,72... | collective-permute-start | bytes 393224 | tf_op jit(solution)/shard_map/ppermute | solution.py:40
  38.3 0.0 collective-permute-done.7
  38.3 1.2 fusion.17
  39.5 0.0 all-to-all-done
  39.5 0.0 copy-start.5
  39.5 3.2 %collective-permute-start.3 = (bf16[512,512]{1,0:T(8,128)(2,1)S(1)}, bf16[512,512]{1,0:T(8,128)(2,1)S(1)}, u32[]{:S(2)}, u32[]{:S(2)}) collective-permute-start(bf16[512,512]{1,0:T(8,128)(2,1)S(1)} %bitcast.57), channel_id=1, source_target_pairs={{0,480},{8,488},{16,496},{24,504},{32,0},{40,8},{48,16},{56,24},{6... | collective-permute-start | bytes 1572872 | tf_op jit(solution)/shard_map/ppermute | solution.py:21
  42.7 2.9 %collective-permute-start.2 = (bf16[512,512]{1,0:T(8,128)(2,1)S(1)}, bf16[512,512]{1,0:T(8,128)(2,1)S(1)}, u32[]{:S(2)}, u32[]{:S(2)}) collective-permute-start(bf16[512,512]{1,0:T(8,128)(2,1)S(1)} %bitcast.58), channel_id=1, source_target_pairs={{0,32},{8,40},{16,48},{24,56},{32,64},{40,72},{48,80},{56,88},{64,... | collective-permute-start | bytes 1572872 | tf_op jit(solution)/shard_map/ppermute | solution.py:21
  45.7 1.5 %fusion.15 = f32[512,512]{1,0:T(8,128)S(1)} fusion(bf16[512,512]{1,0:T(8,128)(2,1)S(1)} %bitcast.59, bf16[512,4096]{1,0:T(8,128)(2,1)} %bitcast.47, u32[]{:T(128)S(6)} %mul.106), kind=kOutput, calls=%fused_computation.20 | convolution fusion | flops 268435456 | bytes 2097156 | tf_op jit(solution)/shard_map/dot_general | solution.py:61
  47.1 1.2 convolution_add_fusion.4
  48.3 6.7 %collective-permute-done.3 = bf16[512,512]{1,0:T(8,128)(2,1)S(1)} collective-permute-done((bf16[512,512]{1,0:T(8,128)(2,1)S(1)}, bf16[512,512]{1,0:T(8,128)(2,1)S(1)}, u32[]{:S(2)}, u32[]{:S(2)}) %collective-permute-start.3) | collective-permute-done | bytes 524320 | tf_op jit(solution)/shard_map/ppermute | solution.py:21
  55.0 5.6 %collective-permute-start.6 = (bf16[512,512]{1,0:T(8,128)(2,1)S(1)}, bf16[512,512]{1,0:T(8,128)(2,1)S(1)}, u32[]{:S(2)}, u32[]{:S(2)}) collective-permute-start(bf16[512,512]{1,0:T(8,128)(2,1)S(1)} %collective-permute-done.3), channel_id=1, source_target_pairs={{0,480},{8,488},{16,496},{24,504},{32,0},{40,8},{48,16},{56,24},{6... | collective-permute-start | bytes 1572872 | tf_op jit(solution)/shard_map/ppermute | solution.py:21
  60.6 0.0 collective-permute-done.2
  60.6 1.9 %collective-permute-start.5 = (bf16[512,512]{1,0:T(8,128)(2,1)S(1)}, bf16[512,512]{1,0:T(8,128)(2,1)S(1)}, u32[]{:S(2)}, u32[]{:S(2)}) collective-permute-start(bf16[512,512]{1,0:T(8,128)(2,1)S(1)} %collective-permute-done.2), channel_id=1, source_target_pairs={{0,32},{8,40},{16,48},{24,56},{32,64},{40,72},{48,80},{56,88},{64,... | collective-permute-start | bytes 1572872 | tf_op jit(solution)/shard_map/ppermute | solution.py:21
  62.5 0.0 copy-done.5
  62.5 0.4 fusion.11
  63.0 0.4 fusion.13
  63.4 8.6 %collective-permute-done.6 = bf16[512,512]{1,0:T(8,128)(2,1)S(1)} collective-permute-done((bf16[512,512]{1,0:T(8,128)(2,1)S(1)}, bf16[512,512]{1,0:T(8,128)(2,1)S(1)}, u32[]{:S(2)}, u32[]{:S(2)}) %collective-permute-start.6) | collective-permute-done | bytes 524320 | tf_op jit(solution)/shard_map/ppermute | solution.py:21
  72.0 5.6 %collective-permute-start.9 = (bf16[512,512]{1,0:T(8,128)(2,1)S(1)}, bf16[512,512]{1,0:T(8,128)(2,1)S(1)}, u32[]{:S(2)}, u32[]{:S(2)}) collective-permute-start(bf16[512,512]{1,0:T(8,128)(2,1)S(1)} %collective-permute-done.6), channel_id=1, source_target_pairs={{0,480},{8,488},{16,496},{24,504},{32,0},{40,8},{48,16},{56,24},{6... | collective-permute-start | bytes 1572872 | tf_op jit(solution)/shard_map/ppermute | solution.py:21
  77.6 0.4 fusion.7
  78.0 0.0 collective-permute-done.5
  78.0 1.9 %collective-permute-start.8 = (bf16[512,512]{1,0:T(8,128)(2,1)S(1)}, bf16[512,512]{1,0:T(8,128)(2,1)S(1)}, u32[]{:S(2)}, u32[]{:S(2)}) collective-permute-start(bf16[512,512]{1,0:T(8,128)(2,1)S(1)} %collective-permute-done.5), channel_id=1, source_target_pairs={{0,32},{8,40},{16,48},{24,56},{32,64},{40,72},{48,80},{56,88},{64,... | collective-permute-start | bytes 1572872 | tf_op jit(solution)/shard_map/ppermute | solution.py:21
  80.0 0.4 fusion.9
  80.4 0.0 collective-permute-done.4
  80.4 0.3 fusion.4
  80.7 0.0 collective-permute-done.1
  80.7 0.3 fusion.3
  81.0 0.0 copy-start
  81.1 0.0 copy-start.1
  81.1 0.0 copy-start.2
  81.1 0.0 copy-start.3
  81.1 12.8 %collective-permute-done.8 = bf16[512,512]{1,0:T(8,128)(2,1)S(1)} collective-permute-done((bf16[512,512]{1,0:T(8,128)(2,1)S(1)}, bf16[512,512]{1,0:T(8,128)(2,1)S(1)}, u32[]{:S(2)}, u32[]{:S(2)}) %collective-permute-start.8) | collective-permute-done | bytes 524320 | tf_op jit(solution)/shard_map/ppermute | solution.py:21
  93.9 0.4 convolution_add_fusion.1
  94.3 0.0 copy-start.4
  94.4 0.0 collective-permute-done.9
  94.4 0.4 fusion.sums_ref
  94.8 2.7 %shard_map.105 = bf16[256,384]{1,0:T(8,128)(2,1)} custom-call(f32[512,512]{1,0:T(8,128)S(1)} %fusion.sums_ref, f32[128,256]{1,0:T(8,128)S(1)} %copy.16.cosine_ref, f32[128,256]{1,0:T(8,128)S(1)} %copy.17.sine_ref, f32[512,4]{1,0:T(8,128)S(1)} %bitcast.41, bf16[256,128]{1,0:T(8,128)(2,1)S(1)} %pad_bitcast_fusion.carried_ref), custom_call_target="tpu_custom_call" | custom-call | tf_op jit(solution)/shard_map/pallas_call | solution.py:220
  97.5 4.0 %all-to-all-start.1 = ((bf16[32,8,384]{2,1,0:T(8,128)(2,1)}), bf16[32,8,384]{2,1,0:T(8,128)(2,1)S(1)}, u32[]{:S(2)}, u32[]{:S(2)}) async-start(bf16[32,8,384]{2,1,0:T(8,128)(2,1)} %bitcast.10), calls=%async_computation.1 | async-start | bytes 393216 | tf_op jit(solution)/shard_map/all_to_all | solution.py:303
  101.6 0.0 copy-done
  101.6 0.0 copy-done.1
  101.6 0.5 shard_map.106
  102.1 14.6 %all-to-all-done.1 = bf16[32,8,384]{2,1,0:T(8,128)(2,1)S(1)} async-done(((bf16[32,8,384]{2,1,0:T(8,128)(2,1)}), bf16[32,8,384]{2,1,0:T(8,128)(2,1)S(1)}, u32[]{:S(2)}, u32[]{:S(2)}) %all-to-all-start.1) | async-done | bytes 196640 | tf_op jit(solution)/shard_map/all_to_all | solution.py:303
  116.7 0.6 shard_map.107
  117.3 21.0 %all_to_all.15 = bf16[32,8,384]{2,1,0:T(8,128)(2,1)S(1)} all-to-all(bf16[32,8,384]{2,1,0:T(8,128)(2,1)S(1)} %bitcast.43), channel_id=1, replica_groups=mesh['gr'=2,'sp'=32,'tp'=8] {'sp'}, dimensions={0} | all-to-all | bytes 393216 | tf_op jit(solution)/shard_map/all_to_all | solution.py:303
  138.3 1.3 shard_map.108
  (15 shorter events, 0.1 us)
Async XLA Ops:
  2.7 36.8 %all-to-all-start = ((bf16[4,128,512]{2,1,0:T(8,128)(2,1)}), bf16[4,128,512]{2,1,0:T(8,128)(2,1)S(1)}, u32[]{:S(2)}, u32[]{:S(2)}) async-start(bf16[4,128,512]{2,1,0:T(8,128)(2,1)} %get-tuple-element.14), calls=%async_computation | async-start | bytes 1048576 | tf_op jit(solution)/shard_map/all_to_all | solution.py:45
  7.2 19.8 %collective-permute-start = (bf16[128,512]{1,0:T(8,128)(2,1)}, bf16[128,512]{1,0:T(8,128)(2,1)S(1)}, u32[]{:S(2)}, u32[]{:S(2)}) collective-permute-start(bf16[128,512]{1,0:T(8,128)(2,1)} %get-tuple-element.15), channel_id=1, source_target_pairs={{0,384},{1,129},{2,386},{3,131},{4,388},{5,133},{6,390},{7,135},{8... | collective-permute-start | bytes 393224 | tf_op jit(solution)/shard_map/ppermute | solution.py:34
  26.9 11.4 %collective-permute-start.7 = (bf16[128,512]{1,0:T(8,128)(2,1)S(1)}, bf16[128,512]{1,0:T(8,128)(2,1)S(1)}, u32[]{:S(2)}, u32[]{:S(2)}) collective-permute-start(bf16[128,512]{1,0:T(8,128)(2,1)S(1)} %collective-permute-done), channel_id=1, source_target_pairs={{0,24},{8,0},{16,8},{24,16},{32,56},{40,32},{48,40},{56,48},{64,88... | collective-permute-start | bytes 393224 | tf_op jit(solution)/shard_map/ppermute | solution.py:40
  32.8 47.6 %collective-permute-start.4 = (bf16[128,512]{1,0:T(8,128)(2,1)S(1)}, bf16[128,512]{1,0:T(8,128)(2,1)S(1)}, u32[]{:S(2)}, u32[]{:S(2)}) collective-permute-start(bf16[128,512]{1,0:T(8,128)(2,1)S(1)} %collective-permute-done), channel_id=1, source_target_pairs={{0,16},{8,24},{16,0},{24,8},{32,48},{40,56},{48,32},{56,40},{64,80... | collective-permute-start | bytes 393224 | tf_op jit(solution)/shard_map/ppermute | solution.py:40
  35.5 45.2 %collective-permute-start.1 = (bf16[128,512]{1,0:T(8,128)(2,1)S(1)}, bf16[128,512]{1,0:T(8,128)(2,1)S(1)}, u32[]{:S(2)}, u32[]{:S(2)}) collective-permute-start(bf16[128,512]{1,0:T(8,128)(2,1)S(1)} %collective-permute-done), channel_id=1, source_target_pairs={{0,8},{8,16},{16,24},{24,0},{32,40},{40,48},{48,56},{56,32},{64,72... | collective-permute-start | bytes 393224 | tf_op jit(solution)/shard_map/ppermute | solution.py:40
  39.5 23.0 %copy-start.5 = (bf16[4,128,4096]{2,1,0:T(8,128)(2,1)S(1)}, bf16[4,128,4096]{2,1,0:T(8,128)(2,1)}, u32[]{:S(2)}) copy-start(bf16[4,128,4096]{2,1,0:T(8,128)(2,1)} %param.9) | copy-start | bytes 12582916
  39.5 15.5 %collective-permute-start.3 = (bf16[512,512]{1,0:T(8,128)(2,1)S(1)}, bf16[512,512]{1,0:T(8,128)(2,1)S(1)}, u32[]{:S(2)}, u32[]{:S(2)}) collective-permute-start(bf16[512,512]{1,0:T(8,128)(2,1)S(1)} %bitcast.57), channel_id=1, source_target_pairs={{0,480},{8,488},{16,496},{24,504},{32,0},{40,8},{48,16},{56,24},{6... | collective-permute-start | bytes 1572872 | tf_op jit(solution)/shard_map/ppermute | solution.py:21
  42.7 17.9 %collective-permute-start.2 = (bf16[512,512]{1,0:T(8,128)(2,1)S(1)}, bf16[512,512]{1,0:T(8,128)(2,1)S(1)}, u32[]{:S(2)}, u32[]{:S(2)}) collective-permute-start(bf16[512,512]{1,0:T(8,128)(2,1)S(1)} %bitcast.58), channel_id=1, source_target_pairs={{0,32},{8,40},{16,48},{24,56},{32,64},{40,72},{48,80},{56,88},{64,... | collective-permute-start | bytes 1572872 | tf_op jit(solution)/shard_map/ppermute | solution.py:21
  55.0 17.0 %collective-permute-start.6 = (bf16[512,512]{1,0:T(8,128)(2,1)S(1)}, bf16[512,512]{1,0:T(8,128)(2,1)S(1)}, u32[]{:S(2)}, u32[]{:S(2)}) collective-permute-start(bf16[512,512]{1,0:T(8,128)(2,1)S(1)} %collective-permute-done.3), channel_id=1, source_target_pairs={{0,480},{8,488},{16,496},{24,504},{32,0},{40,8},{48,16},{56,24},{6... | collective-permute-start | bytes 1572872 | tf_op jit(solution)/shard_map/ppermute | solution.py:21
  60.6 17.4 %collective-permute-start.5 = (bf16[512,512]{1,0:T(8,128)(2,1)S(1)}, bf16[512,512]{1,0:T(8,128)(2,1)S(1)}, u32[]{:S(2)}, u32[]{:S(2)}) collective-permute-start(bf16[512,512]{1,0:T(8,128)(2,1)S(1)} %collective-permute-done.2), channel_id=1, source_target_pairs={{0,32},{8,40},{16,48},{24,56},{32,64},{40,72},{48,80},{56,88},{64,... | collective-permute-start | bytes 1572872 | tf_op jit(solution)/shard_map/ppermute | solution.py:21
  72.0 22.4 %collective-permute-start.9 = (bf16[512,512]{1,0:T(8,128)(2,1)S(1)}, bf16[512,512]{1,0:T(8,128)(2,1)S(1)}, u32[]{:S(2)}, u32[]{:S(2)}) collective-permute-start(bf16[512,512]{1,0:T(8,128)(2,1)S(1)} %collective-permute-done.6), channel_id=1, source_target_pairs={{0,480},{8,488},{16,496},{24,504},{32,0},{40,8},{48,16},{56,24},{6... | collective-permute-start | bytes 1572872 | tf_op jit(solution)/shard_map/ppermute | solution.py:21
  78.0 15.9 %collective-permute-start.8 = (bf16[512,512]{1,0:T(8,128)(2,1)S(1)}, bf16[512,512]{1,0:T(8,128)(2,1)S(1)}, u32[]{:S(2)}, u32[]{:S(2)}) collective-permute-start(bf16[512,512]{1,0:T(8,128)(2,1)S(1)} %collective-permute-done.5), channel_id=1, source_target_pairs={{0,32},{8,40},{16,48},{24,56},{32,64},{40,72},{48,80},{56,88},{64,... | collective-permute-start | bytes 1572872 | tf_op jit(solution)/shard_map/ppermute | solution.py:21
  81.0 20.5 %copy-start = (bf16[4,256]{1,0:T(4,128)(2,1)S(1)}, bf16[4,256]{1,0:T(4,128)(2,1)}, u32[]{:S(2)}) copy-start(bf16[4,256]{1,0:T(4,128)(2,1)} %query_ref.1) | copy-start | bytes 6148
  81.1 20.5 %copy-start.1 = (bf16[4,256]{1,0:T(4,128)(2,1)S(1)}, bf16[4,256]{1,0:T(4,128)(2,1)}, u32[]{:S(2)}) copy-start(bf16[4,256]{1,0:T(4,128)(2,1)} %key_ref.3) | copy-start | bytes 6148
  81.1 20.5 %copy-start.2 = (bf16[4,256]{1,0:T(4,128)(2,1)S(1)}, bf16[4,256]{1,0:T(4,128)(2,1)}, u32[]{:S(2)}) copy-start(bf16[4,256]{1,0:T(4,128)(2,1)} %value_ref.3) | copy-start | bytes 6148
  81.1 20.5 %copy-start.3 = (f32[4,4]{1,0:T(4,128)S(1)}, f32[4,4]{1,0:T(4,128)}, u32[]{:S(2)}) copy-start(f32[4,4]{1,0:T(4,128)} %decay_ref.1) | copy-start | bytes 196
  94.3 44.0 %copy-start.4 = (f32[256]{0:T(256)S(1)}, f32[256]{0:T(256)}, u32[]{:S(2)}) copy-start(f32[256]{0:T(256)} %param.17) | copy-start | bytes 3076
  97.5 19.2 %all-to-all-start.1 = ((bf16[32,8,384]{2,1,0:T(8,128)(2,1)}), bf16[32,8,384]{2,1,0:T(8,128)(2,1)S(1)}, u32[]{:S(2)}, u32[]{:S(2)}) async-start(bf16[32,8,384]{2,1,0:T(8,128)(2,1)} %bitcast.10), calls=%async_computation.1 | async-start | bytes 393216 | tf_op jit(solution)/shard_map/all_to_all | solution.py:303
where the time goes:
time: 140 us
  starting transfers between devices  53 us (38%)
  waiting for transfers between devices  46 us (33%)
  blocking collectives  21 us (15%)
  Pallas kernels  7.2 us (5%)
  matrix products  7.09 us (5%)
  other arithmetic  3.49 us (2%)
    ppermute x6, waiting for transfers between devices, moved_along_z(): return lax.ppermute(x, ('gr', 'sp'), pairs)  28.1 us
    ppermute x6, starting transfers between devices, moved_along_z(): return lax.ppermute(x, ('gr', 'sp'), pairs)  21.1 us
    all_to_all x1, blocking collectives, exchanged(): return lax.all_to_all(cut, 'sp', 0, 0, tiled=True).reshape(x.shape)  21 us
    all_to_all x1, waiting for transfers between devices, exchanged(): return lax.all_to_all(cut, 'sp', 0, 0, tiled=True).reshape(x.shape)  14.6 us
    ppermute x1, starting transfers between devices, from_opposite_plane(): return lax.ppermute(x, ('gr', 'sp', 'tp'), pairs)  12.7 us
    ppermute x3, starting transfers between devices, moved_along_y(): return lax.ppermute(x, 'sp', pairs)  10.7 us
    dot_general x11, matrix products, part(): return jnp.dot(cols, weights, preferred_element_type=F32)  7.09 us
    pallas_call x3, Pallas kernels, in_vmem(): pl.pallas_call(kernel, out_shape=shapes, in_specs=[space] * len(operands)...  4.63 us
  transfers between devices with their start and end apart: 12, of which 5 were waited for; matrix products, arithmetic and copies ran while one was open for 8% of the time, Pallas kernels for 0%

commit v1 on v0

--- a/solution.py
+++ b/solution.py
@@ -92,14 +92,22 @@
     return lax.broadcasted_iota(jnp.int32, shape, 0)
 
 
-def spread_kernel(key_ref, value_ref, own_ref, spread_ref, sems):
+def spread_kernel(key_ref, value_ref, own_ref, spread_ref, in_sems, out_sems):
     cols = key_ref.shape[1]
+    cuts = (pl.ds(0, cols), pl.ds(cols, cols))
+    loads = [
+        pltpu.make_async_copy(ref, own_ref.at[:, cut], in_sems.at[n])
+        for n, (ref, cut) in enumerate(zip((key_ref, value_ref), cuts))
+    ]
+    for load in loads:
+        load.start()
     copies = []
-    for ref, cut in ((key_ref, pl.ds(0, cols)), (value_ref, pl.ds(cols, cols))):
-        for to in (own_ref.at[:, cut], *(spread_ref.at[y, :, cut] for y in range(Y))):
-            copies.append(pltpu.make_async_copy(ref, to, sems.at[len(copies)]))
-    for copy in copies:
-        copy.start()
+    for load, cut in zip(loads, cuts):
+        load.wait()
+        for y in range(Y):
+            to = spread_ref.at[y, :, cut]
+            copies.append(pltpu.make_async_copy(own_ref.at[:, cut], to, out_sems.at[len(copies)]))
+            copies[-1].start()
     for copy in copies:
         copy.wait()
 
@@ -275,8 +283,11 @@
             jax.ShapeDtypeStruct((Y, depth, 2 * cols), BF16),
         ],
         in_specs=[pl.BlockSpec(memory_space=pl.ANY)] * 2,
-        out_specs=[pl.BlockSpec(memory_space=pltpu.VMEM)] * 2,
-        scratch_shapes=[pltpu.SemaphoreType.DMA((2 * (Y + 1),))],
+        out_specs=[
+            pl.BlockSpec(memory_space=pltpu.VMEM),
+            pl.BlockSpec(memory_space=pl.ANY),
+        ],
+        scratch_shapes=[pltpu.SemaphoreType.DMA((2,)), pltpu.SemaphoreType.DMA((2 * Y,))],
     )(key_weight, value_weight)
     sums = projected(tokens.reshape(seqs * span, width), own, spread)
     place = pl.BlockSpec(memory_space=pltpu.SMEM)

time: 140 us -> 141 us (level)
  no operation moved by 1% of the time
where the time goes in v1:
time: 141 us; the launch traced here: 140 us
  starting transfers between devices  53 us (38%)
  waiting for transfers between devices  46 us (33%)
  blocking collectives  21 us (15%)
  Pallas kernels  7.51 us (5%)
  matrix products  7.09 us (5%)
  other arithmetic  3.49 us (2%)
    ppermute x6, waiting for transfers between devices, moved_along_z(): return lax.ppermute(x, ('gr', 'sp'), pairs)  28 us
    ppermute x6, starting transfers between devices, moved_along_z(): return lax.ppermute(x, ('gr', 'sp'), pairs)  21.1 us
    all_to_all x1, blocking collectives, exchanged(): return lax.all_to_all(cut, 'sp', 0, 0, tiled=True).reshape(x.shape)  21 us
    all_to_all x1, waiting for transfers between devices, exchanged(): return lax.all_to_all(cut, 'sp', 0, 0, tiled=True).reshape(x.shape)  14.6 us
    ppermute x1, starting transfers between devices, from_opposite_plane(): return lax.ppermute(x, ('gr', 'sp', 'tp'), pairs)  12.7 us
    ppermute x3, starting transfers between devices, moved_along_y(): return lax.ppermute(x, 'sp', pairs)  10.7 us
    dot_general x11, matrix products, part(): return jnp.dot(cols, weights, preferred_element_type=F32)  7.09 us
    pallas_call x3, Pallas kernels, in_vmem(): pl.pallas_call(kernel, out_shape=shapes, in_specs=[space] * len(operands)...  4.62 us
  transfers between devices with their start and end apart: 12, of which 5 were waited for; matrix products, arithmetic and copies ran while one was open for 8% of the time, Pallas kernels for 0%

profile of v1, /device:TPU:2, one launch (start us, length us, event | category | flops | bytes accessed | tf_op | source)
XLA Modules:
  0.0 139.9 jit_solution(9112684363351923505)
XLA Ops:
  0.6 2.4 %shard_map.104 = (bf16[128,512]{1,0:T(8,128)(2,1)}, bf16[4,128,512]{2,1,0:T(8,128)(2,1)}) custom-call(bf16[128,256]{1,0:T(8,128)(2,1)} %key_ref.2, bf16[128,256]{1,0:T(8,128)(2,1)} %value_ref.2), custom_call_target="tpu_custom_call" | custom-call | tf_op jit(solution)/shard_map/pallas_call | solution.py:279
  3.0 4.5 %all-to-all-start = ((bf16[4,128,512]{2,1,0:T(8,128)(2,1)}), bf16[4,128,512]{2,1,0:T(8,128)(2,1)S(1)}, u32[]{:S(2)}, u32[]{:S(2)}) async-start(bf16[4,128,512]{2,1,0:T(8,128)(2,1)} %get-tuple-element.14), calls=%async_computation | async-start | bytes 1048576 | tf_op jit(solution)/shard_map/all_to_all | solution.py:45
  7.5 12.7 %collective-permute-start = (bf16[128,512]{1,0:T(8,128)(2,1)}, bf16[128,512]{1,0:T(8,128)(2,1)S(1)}, u32[]{:S(2)}, u32[]{:S(2)}) collective-permute-start(bf16[128,512]{1,0:T(8,128)(2,1)} %get-tuple-element.15), channel_id=1, source_target_pairs={{0,384},{1,129},{2,386},{3,131},{4,388},{5,133},{6,390},{7,135},{8... | collective-permute-start | bytes 393224 | tf_op jit(solution)/shard_map/ppermute | solution.py:34
  20.2 0.1 multiply_sine_fusion.1
  20.3 0.8 reduce_sum.11
  21.1 2.3 %reduce_window_sum.13 = f32[4,4,128]{2,1,0:T(4,128)S(1)} reduce-window(f32[4,4,128]{2,1,0:T(4,128)} %param.12, f32[]{:T(128)} %constant.121.clone.1), window={size=1x1x128 pad=0_0x0_0x127_0}, to_apply=%region_1.0 | reduce-window | flops 260096 | bytes 16388 | tf_op jit(solution)/shard_map/jit(cumsum)/reduce_window_sum | solution.py:263
  23.4 0.1 copy.14
  23.5 0.1 broadcast_in_dim.15
  23.6 0.1 fusion.25
  23.7 0.1 fusion.24
  23.8 0.1 multiply_cosine_fusion.1
  23.9 3.4 %collective-permute-done = bf16[128,512]{1,0:T(8,128)(2,1)S(1)} collective-permute-done((bf16[128,512]{1,0:T(8,128)(2,1)}, bf16[128,512]{1,0:T(8,128)(2,1)S(1)}, u32[]{:S(2)}, u32[]{:S(2)}) %collective-permute-start) | collective-permute-done | bytes 131104 | tf_op jit(solution)/shard_map/ppermute | solution.py:34
  27.2 5.1 %collective-permute-start.7 = (bf16[128,512]{1,0:T(8,128)(2,1)S(1)}, bf16[128,512]{1,0:T(8,128)(2,1)S(1)}, u32[]{:S(2)}, u32[]{:S(2)}) collective-permute-start(bf16[128,512]{1,0:T(8,128)(2,1)S(1)} %collective-permute-done), channel_id=1, source_target_pairs={{0,24},{8,0},{16,8},{24,16},{32,56},{40,32},{48,40},{56,48},{64,88... | collective-permute-start | bytes 393224 | tf_op jit(solution)/shard_map/ppermute | solution.py:40
  32.4 0.1 pad_maximum_fusion.2
  32.5 0.1 broadcast_in_dim_tile.7.sine_ref
  32.6 0.1 copy.13
  32.7 0.1 broadcast_in_dim_tile.6.cosine_ref
  32.9 0.1 copy.16.cosine_ref
  33.0 0.1 copy.17.sine_ref
  33.1 2.8 %collective-permute-start.4 = (bf16[128,512]{1,0:T(8,128)(2,1)S(1)}, bf16[128,512]{1,0:T(8,128)(2,1)S(1)}, u32[]{:S(2)}, u32[]{:S(2)}) collective-permute-start(bf16[128,512]{1,0:T(8,128)(2,1)S(1)} %collective-permute-done), channel_id=1, source_target_pairs={{0,16},{8,24},{16,0},{24,8},{32,48},{40,56},{48,32},{56,40},{64,80... | collective-permute-start | bytes 393224 | tf_op jit(solution)/shard_map/ppermute | solution.py:40
  35.9 2.8 %collective-permute-start.1 = (bf16[128,512]{1,0:T(8,128)(2,1)S(1)}, bf16[128,512]{1,0:T(8,128)(2,1)S(1)}, u32[]{:S(2)}, u32[]{:S(2)}) collective-permute-start(bf16[128,512]{1,0:T(8,128)(2,1)S(1)} %collective-permute-done), channel_id=1, source_target_pairs={{0,8},{8,16},{16,24},{24,0},{32,40},{40,48},{48,56},{56,32},{64,72... | collective-permute-start | bytes 393224 | tf_op jit(solution)/shard_map/ppermute | solution.py:40
  38.6 0.0 collective-permute-done.7
  38.6 1.2 fusion.17
  39.8 0.0 all-to-all-done
  39.8 0.0 copy-start.5
  39.9 3.2 %collective-permute-start.3 = (bf16[512,512]{1,0:T(8,128)(2,1)S(1)}, bf16[512,512]{1,0:T(8,128)(2,1)S(1)}, u32[]{:S(2)}, u32[]{:S(2)}) collective-permute-start(bf16[512,512]{1,0:T(8,128)(2,1)S(1)} %bitcast.57), channel_id=1, source_target_pairs={{0,480},{8,488},{16,496},{24,504},{32,0},{40,8},{48,16},{56,24},{6... | collective-permute-start | bytes 1572872 | tf_op jit(solution)/shard_map/ppermute | solution.py:21
  43.0 2.9 %collective-permute-start.2 = (bf16[512,512]{1,0:T(8,128)(2,1)S(1)}, bf16[512,512]{1,0:T(8,128)(2,1)S(1)}, u32[]{:S(2)}, u32[]{:S(2)}) collective-permute-start(bf16[512,512]{1,0:T(8,128)(2,1)S(1)} %bitcast.58), channel_id=1, source_target_pairs={{0,32},{8,40},{16,48},{24,56},{32,64},{40,72},{48,80},{56,88},{64,... | collective-permute-start | bytes 1572872 | tf_op jit(solution)/shard_map/ppermute | solution.py:21
  46.0 1.5 %fusion.15 = f32[512,512]{1,0:T(8,128)S(1)} fusion(bf16[512,512]{1,0:T(8,128)(2,1)S(1)} %bitcast.59, bf16[512,4096]{1,0:T(8,128)(2,1)} %bitcast.47, u32[]{:T(128)S(6)} %mul.106), kind=kOutput, calls=%fused_computation.20 | convolution fusion | flops 268435456 | bytes 2097156 | tf_op jit(solution)/shard_map/dot_general | solution.py:61
  47.5 1.2 convolution_add_fusion.4
  48.6 6.7 %collective-permute-done.3 = bf16[512,512]{1,0:T(8,128)(2,1)S(1)} collective-permute-done((bf16[512,512]{1,0:T(8,128)(2,1)S(1)}, bf16[512,512]{1,0:T(8,128)(2,1)S(1)}, u32[]{:S(2)}, u32[]{:S(2)}) %collective-permute-start.3) | collective-permute-done | bytes 524320 | tf_op jit(solution)/shard_map/ppermute | solution.py:21
  55.3 5.6 %collective-permute-start.6 = (bf16[512,512]{1,0:T(8,128)(2,1)S(1)}, bf16[512,512]{1,0:T(8,128)(2,1)S(1)}, u32[]{:S(2)}, u32[]{:S(2)}) collective-permute-start(bf16[512,512]{1,0:T(8,128)(2,1)S(1)} %collective-permute-done.3), channel_id=1, source_target_pairs={{0,480},{8,488},{16,496},{24,504},{32,0},{40,8},{48,16},{56,24},{6... | collective-permute-start | bytes 1572872 | tf_op jit(solution)/shard_map/ppermute | solution.py:21
  60.9 0.0 collective-permute-done.2
  60.9 1.9 %collective-permute-start.5 = (bf16[512,512]{1,0:T(8,128)(2,1)S(1)}, bf16[512,512]{1,0:T(8,128)(2,1)S(1)}, u32[]{:S(2)}, u32[]{:S(2)}) collective-permute-start(bf16[512,512]{1,0:T(8,128)(2,1)S(1)} %collective-permute-done.2), channel_id=1, source_target_pairs={{0,32},{8,40},{16,48},{24,56},{32,64},{40,72},{48,80},{56,88},{64,... | collective-permute-start | bytes 1572872 | tf_op jit(solution)/shard_map/ppermute | solution.py:21
  62.8 0.0 copy-done.5
  62.8 0.4 fusion.11
  63.3 0.4 fusion.13
  63.7 8.6 %collective-permute-done.6 = bf16[512,512]{1,0:T(8,128)(2,1)S(1)} collective-permute-done((bf16[512,512]{1,0:T(8,128)(2,1)S(1)}, bf16[512,512]{1,0:T(8,128)(2,1)S(1)}, u32[]{:S(2)}, u32[]{:S(2)}) %collective-permute-start.6) | collective-permute-done | bytes 524320 | tf_op jit(solution)/shard_map/ppermute | solution.py:21
  72.3 5.6 %collective-permute-start.9 = (bf16[512,512]{1,0:T(8,128)(2,1)S(1)}, bf16[512,512]{1,0:T(8,128)(2,1)S(1)}, u32[]{:S(2)}, u32[]{:S(2)}) collective-permute-start(bf16[512,512]{1,0:T(8,128)(2,1)S(1)} %collective-permute-done.6), channel_id=1, source_target_pairs={{0,480},{8,488},{16,496},{24,504},{32,0},{40,8},{48,16},{56,24},{6... | collective-permute-start | bytes 1572872 | tf_op jit(solution)/shard_map/ppermute | solution.py:21
  77.9 0.4 fusion.7
  78.3 0.0 collective-permute-done.5
  78.3 1.9 %collective-permute-start.8 = (bf16[512,512]{1,0:T(8,128)(2,1)S(1)}, bf16[512,512]{1,0:T(8,128)(2,1)S(1)}, u32[]{:S(2)}, u32[]{:S(2)}) collective-permute-start(bf16[512,512]{1,0:T(8,128)(2,1)S(1)} %collective-permute-done.5), channel_id=1, source_target_pairs={{0,32},{8,40},{16,48},{24,56},{32,64},{40,72},{48,80},{56,88},{64,... | collective-permute-start | bytes 1572872 | tf_op jit(solution)/shard_map/ppermute | solution.py:21
  80.3 0.4 fusion.9
  80.7 0.0 collective-permute-done.4
  80.7 0.3 fusion.4
  81.0 0.0 collective-permute-done.1
  81.0 0.3 fusion.3
  81.3 0.0 copy-start
  81.4 0.0 copy-start.1
  81.4 0.0 copy-start.2
  81.4 0.0 copy-start.3
  81.4 12.8 %collective-permute-done.8 = bf16[512,512]{1,0:T(8,128)(2,1)S(1)} collective-permute-done((bf16[512,512]{1,0:T(8,128)(2,1)S(1)}, bf16[512,512]{1,0:T(8,128)(2,1)S(1)}, u32[]{:S(2)}, u32[]{:S(2)}) %collective-permute-start.8) | collective-permute-done | bytes 524320 | tf_op jit(solution)/shard_map/ppermute | solution.py:21
  94.2 0.4 convolution_add_fusion.1
  94.6 0.0 copy-start.4
  94.7 0.0 collective-permute-done.9
  94.7 0.4 fusion.sums_ref
  95.1 2.7 %shard_map.105 = bf16[256,384]{1,0:T(8,128)(2,1)} custom-call(f32[512,512]{1,0:T(8,128)S(1)} %fusion.sums_ref, f32[128,256]{1,0:T(8,128)S(1)} %copy.16.cosine_ref, f32[128,256]{1,0:T(8,128)S(1)} %copy.17.sine_ref, f32[512,4]{1,0:T(8,128)S(1)} %bitcast.41, bf16[256,128]{1,0:T(8,128)(2,1)S(1)} %pad_bitcast_fusion.carried_ref), custom_call_target="tpu_custom_call" | custom-call | tf_op jit(solution)/shard_map/pallas_call | solution.py:228
  97.8 4.0 %all-to-all-start.1 = ((bf16[32,8,384]{2,1,0:T(8,128)(2,1)}), bf16[32,8,384]{2,1,0:T(8,128)(2,1)S(1)}, u32[]{:S(2)}, u32[]{:S(2)}) async-start(bf16[32,8,384]{2,1,0:T(8,128)(2,1)} %bitcast.10), calls=%async_computation.1 | async-start | bytes 393216 | tf_op jit(solution)/shard_map/all_to_all | solution.py:314
  101.9 0.0 copy-done
  101.9 0.0 copy-done.1
  101.9 0.5 shard_map.106
  102.4 14.6 %all-to-all-done.1 = bf16[32,8,384]{2,1,0:T(8,128)(2,1)S(1)} async-done(((bf16[32,8,384]{2,1,0:T(8,128)(2,1)}), bf16[32,8,384]{2,1,0:T(8,128)(2,1)S(1)}, u32[]{:S(2)}, u32[]{:S(2)}) %all-to-all-start.1) | async-done | bytes 196640 | tf_op jit(solution)/shard_map/all_to_all | solution.py:314
  117.0 0.6 shard_map.107
  117.6 21.0 %all_to_all.15 = bf16[32,8,384]{2,1,0:T(8,128)(2,1)S(1)} all-to-all(bf16[32,8,384]{2,1,0:T(8,128)(2,1)S(1)} %bitcast.43), channel_id=1, replica_groups=mesh['gr'=2,'sp'=32,'tp'=8] {'sp'}, dimensions={0} | all-to-all | bytes 393216 | tf_op jit(solution)/shard_map/all_to_all | solution.py:314
  138.6 1.3 shard_map.108
  (15 shorter events, 0.1 us)
Async XLA Ops:
  3.0 36.8 %all-to-all-start = ((bf16[4,128,512]{2,1,0:T(8,128)(2,1)}), bf16[4,128,512]{2,1,0:T(8,128)(2,1)S(1)}, u32[]{:S(2)}, u32[]{:S(2)}) async-start(bf16[4,128,512]{2,1,0:T(8,128)(2,1)} %get-tuple-element.14), calls=%async_computation | async-start | bytes 1048576 | tf_op jit(solution)/shard_map/all_to_all | solution.py:45
  7.5 19.8 %collective-permute-start = (bf16[128,512]{1,0:T(8,128)(2,1)}, bf16[128,512]{1,0:T(8,128)(2,1)S(1)}, u32[]{:S(2)}, u32[]{:S(2)}) collective-permute-start(bf16[128,512]{1,0:T(8,128)(2,1)} %get-tuple-element.15), channel_id=1, source_target_pairs={{0,384},{1,129},{2,386},{3,131},{4,388},{5,133},{6,390},{7,135},{8... | collective-permute-start | bytes 393224 | tf_op jit(solution)/shard_map/ppermute | solution.py:34
  27.2 11.4 %collective-permute-start.7 = (bf16[128,512]{1,0:T(8,128)(2,1)S(1)}, bf16[128,512]{1,0:T(8,128)(2,1)S(1)}, u32[]{:S(2)}, u32[]{:S(2)}) collective-permute-start(bf16[128,512]{1,0:T(8,128)(2,1)S(1)} %collective-permute-done), channel_id=1, source_target_pairs={{0,24},{8,0},{16,8},{24,16},{32,56},{40,32},{48,40},{56,48},{64,88... | collective-permute-start | bytes 393224 | tf_op jit(solution)/shard_map/ppermute | solution.py:40
  33.1 47.6 %collective-permute-start.4 = (bf16[128,512]{1,0:T(8,128)(2,1)S(1)}, bf16[128,512]{1,0:T(8,128)(2,1)S(1)}, u32[]{:S(2)}, u32[]{:S(2)}) collective-permute-start(bf16[128,512]{1,0:T(8,128)(2,1)S(1)} %collective-permute-done), channel_id=1, source_target_pairs={{0,16},{8,24},{16,0},{24,8},{32,48},{40,56},{48,32},{56,40},{64,80... | collective-permute-start | bytes 393224 | tf_op jit(solution)/shard_map/ppermute | solution.py:40
  35.9 45.1 %collective-permute-start.1 = (bf16[128,512]{1,0:T(8,128)(2,1)S(1)}, bf16[128,512]{1,0:T(8,128)(2,1)S(1)}, u32[]{:S(2)}, u32[]{:S(2)}) collective-permute-start(bf16[128,512]{1,0:T(8,128)(2,1)S(1)} %collective-permute-done), channel_id=1, source_target_pairs={{0,8},{8,16},{16,24},{24,0},{32,40},{40,48},{48,56},{56,32},{64,72... | collective-permute-start | bytes 393224 | tf_op jit(solution)/shard_map/ppermute | solution.py:40
  39.8 23.0 %copy-start.5 = (bf16[4,128,4096]{2,1,0:T(8,128)(2,1)S(1)}, bf16[4,128,4096]{2,1,0:T(8,128)(2,1)}, u32[]{:S(2)}) copy-start(bf16[4,128,4096]{2,1,0:T(8,128)(2,1)} %param.9) | copy-start | bytes 12582916
  39.9 15.5 %collective-permute-start.3 = (bf16[512,512]{1,0:T(8,128)(2,1)S(1)}, bf16[512,512]{1,0:T(8,128)(2,1)S(1)}, u32[]{:S(2)}, u32[]{:S(2)}) collective-permute-start(bf16[512,512]{1,0:T(8,128)(2,1)S(1)} %bitcast.57), channel_id=1, source_target_pairs={{0,480},{8,488},{16,496},{24,504},{32,0},{40,8},{48,16},{56,24},{6... | collective-permute-start | bytes 1572872 | tf_op jit(solution)/shard_map/ppermute | solution.py:21
  43.0 17.9 %collective-permute-start.2 = (bf16[512,512]{1,0:T(8,128)(2,1)S(1)}, bf16[512,512]{1,0:T(8,128)(2,1)S(1)}, u32[]{:S(2)}, u32[]{:S(2)}) collective-permute-start(bf16[512,512]{1,0:T(8,128)(2,1)S(1)} %bitcast.58), channel_id=1, source_target_pairs={{0,32},{8,40},{16,48},{24,56},{32,64},{40,72},{48,80},{56,88},{64,... | collective-permute-start | bytes 1572872 | tf_op jit(solution)/shard_map/ppermute | solution.py:21
  55.3 17.0 %collective-permute-start.6 = (bf16[512,512]{1,0:T(8,128)(2,1)S(1)}, bf16[512,512]{1,0:T(8,128)(2,1)S(1)}, u32[]{:S(2)}, u32[]{:S(2)}) collective-permute-start(bf16[512,512]{1,0:T(8,128)(2,1)S(1)} %collective-permute-done.3), channel_id=1, source_target_pairs={{0,480},{8,488},{16,496},{24,504},{32,0},{40,8},{48,16},{56,24},{6... | collective-permute-start | bytes 1572872 | tf_op jit(solution)/shard_map/ppermute | solution.py:21
  60.9 17.4 %collective-permute-start.5 = (bf16[512,512]{1,0:T(8,128)(2,1)S(1)}, bf16[512,512]{1,0:T(8,128)(2,1)S(1)}, u32[]{:S(2)}, u32[]{:S(2)}) collective-permute-start(bf16[512,512]{1,0:T(8,128)(2,1)S(1)} %collective-permute-done.2), channel_id=1, source_target_pairs={{0,32},{8,40},{16,48},{24,56},{32,64},{40,72},{48,80},{56,88},{64,... | collective-permute-start | bytes 1572872 | tf_op jit(solution)/shard_map/ppermute | solution.py:21
  72.3 22.4 %collective-permute-start.9 = (bf16[512,512]{1,0:T(8,128)(2,1)S(1)}, bf16[512,512]{1,0:T(8,128)(2,1)S(1)}, u32[]{:S(2)}, u32[]{:S(2)}) collective-permute-start(bf16[512,512]{1,0:T(8,128)(2,1)S(1)} %collective-permute-done.6), channel_id=1, source_target_pairs={{0,480},{8,488},{16,496},{24,504},{32,0},{40,8},{48,16},{56,24},{6... | collective-permute-start | bytes 1572872 | tf_op jit(solution)/shard_map/ppermute | solution.py:21
  78.3 15.9 %collective-permute-start.8 = (bf16[512,512]{1,0:T(8,128)(2,1)S(1)}, bf16[512,512]{1,0:T(8,128)(2,1)S(1)}, u32[]{:S(2)}, u32[]{:S(2)}) collective-permute-start(bf16[512,512]{1,0:T(8,128)(2,1)S(1)} %collective-permute-done.5), channel_id=1, source_target_pairs={{0,32},{8,40},{16,48},{24,56},{32,64},{40,72},{48,80},{56,88},{64,... | collective-permute-start | bytes 1572872 | tf_op jit(solution)/shard_map/ppermute | solution.py:21
  81.3 20.5 %copy-start = (bf16[4,256]{1,0:T(4,128)(2,1)S(1)}, bf16[4,256]{1,0:T(4,128)(2,1)}, u32[]{:S(2)}) copy-start(bf16[4,256]{1,0:T(4,128)(2,1)} %query_ref.1) | copy-start | bytes 6148
  81.4 20.5 %copy-start.1 = (bf16[4,256]{1,0:T(4,128)(2,1)S(1)}, bf16[4,256]{1,0:T(4,128)(2,1)}, u32[]{:S(2)}) copy-start(bf16[4,256]{1,0:T(4,128)(2,1)} %key_ref.3) | copy-start | bytes 6148
  81.4 20.5 %copy-start.2 = (bf16[4,256]{1,0:T(4,128)(2,1)S(1)}, bf16[4,256]{1,0:T(4,128)(2,1)}, u32[]{:S(2)}) copy-start(bf16[4,256]{1,0:T(4,128)(2,1)} %value_ref.3) | copy-start | bytes 6148
  81.4 20.5 %copy-start.3 = (f32[4,4]{1,0:T(4,128)S(1)}, f32[4,4]{1,0:T(4,128)}, u32[]{:S(2)}) copy-start(f32[4,4]{1,0:T(4,128)} %decay_ref.1) | copy-start | bytes 196
  94.6 44.0 %copy-start.4 = (f32[256]{0:T(256)S(1)}, f32[256]{0:T(256)}, u32[]{:S(2)}) copy-start(f32[256]{0:T(256)} %param.17) | copy-start | bytes 3076
  97.8 19.2 %all-to-all-start.1 = ((bf16[32,8,384]{2,1,0:T(8,128)(2,1)}), bf16[32,8,384]{2,1,0:T(8,128)(2,1)S(1)}, u32[]{:S(2)}, u32[]{:S(2)}) async-start(bf16[32,8,384]{2,1,0:T(8,128)(2,1)} %bitcast.10), calls=%async_computation.1 | async-start | bytes 393216 | tf_op jit(solution)/shard_map/all_to_all | solution.py:314

commit v2 on v0

--- a/solution.py
+++ b/solution.py
@@ -104,21 +104,19 @@
         copy.wait()
 
 
-def share_kernel(seqs, sums_ref, cosine_ref, sine_ref, weight_ref, carried_ref, out_ref):
+def share_kernel(seqs, sums_ref, cosine_ref, sine_ref, carried_ref, out_ref):
     cols = out_ref.shape[0]
     heads = cols // HEAD_DIM
     span = sums_ref.shape[0] // seqs
     half = HEAD_DIM // 2
     low = lanes_of((span, cols)) % HEAD_DIM < half
-    spread = (rows_of((heads, cols)) == lanes_of((heads, cols)) // HEAD_DIM).astype(F32)
     blocks = [[] for _ in range(heads)]
     for seq in range(seqs):
         here = pl.ds(seq * span, span)
         keys = sums_ref[here, :cols].astype(BF16).astype(F32)
         values = sums_ref[here, cols:].astype(BF16)
         other = jnp.where(low, pltpu.roll(keys, cols - half, 1), pltpu.roll(keys, half, 1))
-        turned = keys * cosine_ref[...] + other * sine_ref[...]
-        faded = turned * jnp.dot(weight_ref[here, :], spread, precision=EXACT)
+        faded = keys * cosine_ref[here, :] + other * sine_ref[here, :]
         high = faded.astype(BF16)
         rest = (faded - high.astype(F32)).astype(BF16)
         product = sum(
@@ -137,9 +135,29 @@
 
 
 def lines_kernel(
-    place_ref, cosine_ref, sine_ref, query_ref, key_ref, value_ref, decay_ref, lines_ref, values_ref
+    place_ref,
+    cosine_ref,
+    sine_ref,
+    query_ref,
+    key_ref,
+    value_ref,
+    decay_ref,
+    table_cosine_ref,
+    table_sine_ref,
+    weight_ref,
+    lines_ref,
+    values_ref,
+    faded_cosine_ref,
+    faded_sine_ref,
 ):
     seqs, cols = query_ref.shape
+    span = table_cosine_ref.shape[0]
+    spread = (rows_of((cols // HEAD_DIM, cols)) == lanes_of((cols // HEAD_DIM, cols)) // HEAD_DIM)
+    for seq in range(seqs):
+        there = pl.ds(seq * span, span)
+        weight = jnp.dot(weight_ref[there, :], spread.astype(F32), precision=EXACT)
+        faded_cosine_ref[there, :] = table_cosine_ref[...] * weight
+        faded_sine_ref[there, :] = table_sine_ref[...] * weight
     heads, lanes = (cols // HEAD_DIM, seqs * HEAD_DIM)
     rows, half = (values_ref.shape[0], HEAD_DIM // 2)
     mine = place_ref[0]
@@ -281,12 +299,17 @@
     sums = projected(tokens.reshape(seqs * span, width), own, spread)
     place = pl.BlockSpec(memory_space=pltpu.SMEM)
     space = pl.BlockSpec(memory_space=pltpu.VMEM)
-    lines, value_rows = pl.pallas_call(
+    lines, value_rows, cosine, sine = pl.pallas_call(
         lines_kernel,
-        out_shape=[jax.ShapeDtypeStruct((3, lanes), F32), jax.ShapeDtypeStruct((rows, lanes), F32)],
-        in_specs=[place] + [space] * 6,
-        out_specs=[space] * 2,
-        compiler_params=pltpu.CompilerParams(vmem_limit_bytes=2 * 2**20),
+        out_shape=[
+            jax.ShapeDtypeStruct((3, lanes), F32),
+            jax.ShapeDtypeStruct((rows, lanes), F32),
+            jax.ShapeDtypeStruct((seqs * span, cols), F32),
+            jax.ShapeDtypeStruct((seqs * span, cols), F32),
+        ],
+        in_specs=[place] + [space] * 9,
+        out_specs=[space] * 4,
+        compiler_params=pltpu.CompilerParams(vmem_limit_bytes=6 * 2**20),
     )(
         mine[None],
         last_cosine,
@@ -295,6 +318,9 @@
         new_key,
         new_value,
         step_decay,
+        cosine,
+        sine,
+        weight,
     )
     whole = jax.ShapeDtypeStruct((cols, lanes + EXTRA), BF16)
 
@@ -303,7 +329,7 @@
         return lax.all_to_all(cut, "sp", 0, 0, tiled=True).reshape(x.shape)
 
     sent = in_vmem(
-        functools.partial(share_kernel, seqs), whole, sums, cosine, sine, weight, carried
+        functools.partial(share_kernel, seqs), whole, sums, cosine, sine, carried
     )
     finished = in_vmem(
         functools.partial(owner_kernel, devices, seqs), whole, exchanged(sent), lines, value_rows

time: 140 us -> 142 us (1.014)
  blocking collectives: 21 us -> 39.7 us
  waiting for transfers between devices: 46 us -> 31.4 us
  starting transfers between devices: 53 us -> 49 us
  local copies, waits for them, and re-layouts: 0.82 us -> 3.51 us
  Pallas kernels: 7.2 us -> 5.57 us
    all_to_all x1 -> x2, blocking collectives: 21 us -> 39.7 us  [exchanged(): return lax.all_to_all(cut, 'sp', 0, 0, tiled=True).reshape(x.shape)]
    all_to_all x1 -> x0, waiting for transfers between devices: 14.6 us -> none  [exchanged(): return lax.all_to_all(cut, 'sp', 0, 0, tiled=True).reshape(x.shape)]
    all_to_all x1 -> x0, starting transfers between devices: 4.03 us -> none  [exchanged(): return lax.all_to_all(cut, 'sp', 0, 0, tiled=True).reshape(x.shape)]
    unnamed x13, local copies, waits for them, and re-layouts: 0.05 us -> 2.75 us
    pallas_call x3, Pallas kernels: 4.63 us -> 2.59 us  [in_vmem(): pl.pallas_call(kernel, out_shape=shapes, in_specs=[space] * len(operands)...]
  transfers between devices with their start and end apart: 12 -> 11, of which waited for: 5 -> 4; matrix products, arithmetic and copies ran while one was open for 8% -> 8% of each run, Pallas kernels for 0% -> 1%
where the time goes in v2:
time: 142 us; the launch traced here: 141 us
  starting transfers between devices  49 us (35%)
  blocking collectives  39.7 us (28%)
  waiting for transfers between devices  31.4 us (22%)
  matrix products  7.1 us (5%)
  Pallas kernels  5.57 us (4%)
  local copies, waits for them, and re-layouts  3.51 us (2%)
  other arithmetic  3.49 us (2%)
    all_to_all x2, blocking collectives, exchanged(): return lax.all_to_all(cut, 'sp', 0, 0, tiled=True).reshape(x.shape)  39.7 us
    ppermute x6, waiting for transfers between devices, moved_along_z(): return lax.ppermute(x, ('gr', 'sp'), pairs)  28.1 us
    ppermute x6, starting transfers between devices, moved_along_z(): return lax.ppermute(x, ('gr', 'sp'), pairs)  21.1 us
    ppermute x1, starting transfers between devices, from_opposite_plane(): return lax.ppermute(x, ('gr', 'sp', 'tp'), pairs)  12.7 us
    ppermute x3, starting transfers between devices, moved_along_y(): return lax.ppermute(x, 'sp', pairs)  10.7 us
    dot_general x11, matrix products, part(): return jnp.dot(cols, weights, preferred_element_type=F32)  7.1 us
    all_to_all x1, starting transfers between devices, exchanged_along_y(): lax.all_to_all(spread, 'sp', 0, 0, tiled=True, axis_index_groups=groups)  4.48 us
    ppermute x1, waiting for transfers between devices, from_opposite_plane(): return lax.ppermute(x, ('gr', 'sp', 'tp'), pairs)  3.36 us
  transfers between devices with their start and end apart: 11, of which 4 were waited for; matrix products, arithmetic and copies ran while one was open for 8% of the time, Pallas kernels for 1%

profile of v2, /device:TPU:2, one launch (start us, length us, event | category | flops | bytes accessed | tf_op | source)
XLA Modules:
  0.0 140.8 jit_solution(13469434427323163824)
XLA Ops:
  0.6 2.1 %shard_map.104 = (bf16[128,512]{1,0:T(8,128)(2,1)}, bf16[4,128,512]{2,1,0:T(8,128)(2,1)}) custom-call(bf16[128,256]{1,0:T(8,128)(2,1)} %key_ref.2, bf16[128,256]{1,0:T(8,128)(2,1)} %value_ref.2), custom_call_target="tpu_custom_call" | custom-call | tf_op jit(solution)/shard_map/pallas_call | solution.py:289
  2.7 4.5 %all-to-all-start = ((bf16[4,128,512]{2,1,0:T(8,128)(2,1)}), bf16[4,128,512]{2,1,0:T(8,128)(2,1)S(1)}, u32[]{:S(2)}, u32[]{:S(2)}) async-start(bf16[4,128,512]{2,1,0:T(8,128)(2,1)} %get-tuple-element.16), calls=%async_computation | async-start | bytes 1048576 | tf_op jit(solution)/shard_map/all_to_all | solution.py:45
  7.2 12.7 %collective-permute-start = (bf16[128,512]{1,0:T(8,128)(2,1)}, bf16[128,512]{1,0:T(8,128)(2,1)S(1)}, u32[]{:S(2)}, u32[]{:S(2)}) collective-permute-start(bf16[128,512]{1,0:T(8,128)(2,1)} %get-tuple-element.17), channel_id=1, source_target_pairs={{0,384},{1,129},{2,386},{3,131},{4,388},{5,133},{6,390},{7,135},{8... | collective-permute-start | bytes 393224 | tf_op jit(solution)/shard_map/ppermute | solution.py:34
  19.9 0.1 multiply_sine_fusion.1
  20.0 0.8 reduce_sum.11
  20.8 2.3 %reduce_window_sum.13 = f32[4,4,128]{2,1,0:T(4,128)S(1)} reduce-window(f32[4,4,128]{2,1,0:T(4,128)} %param.12, f32[]{:T(128)} %constant.121.clone.1), window={size=1x1x128 pad=0_0x0_0x127_0}, to_apply=%region_1.0 | reduce-window | flops 260096 | bytes 16388 | tf_op jit(solution)/shard_map/jit(cumsum)/reduce_window_sum | solution.py:273
  23.1 0.1 copy.14
  23.2 0.1 broadcast_in_dim.16
  23.3 0.1 fusion.25
  23.4 0.1 fusion.24
  23.5 0.1 multiply_cosine_fusion.1
  23.6 3.4 %collective-permute-done = bf16[128,512]{1,0:T(8,128)(2,1)S(1)} collective-permute-done((bf16[128,512]{1,0:T(8,128)(2,1)}, bf16[128,512]{1,0:T(8,128)(2,1)S(1)}, u32[]{:S(2)}, u32[]{:S(2)}) %collective-permute-start) | collective-permute-done | bytes 131104 | tf_op jit(solution)/shard_map/ppermute | solution.py:34
  26.9 5.1 %collective-permute-start.7 = (bf16[128,512]{1,0:T(8,128)(2,1)S(1)}, bf16[128,512]{1,0:T(8,128)(2,1)S(1)}, u32[]{:S(2)}, u32[]{:S(2)}) collective-permute-start(bf16[128,512]{1,0:T(8,128)(2,1)S(1)} %collective-permute-done), channel_id=1, source_target_pairs={{0,24},{8,0},{16,8},{24,16},{32,56},{40,32},{48,40},{56,48},{64,88... | collective-permute-start | bytes 393224 | tf_op jit(solution)/shard_map/ppermute | solution.py:40
  32.1 0.1 pad_maximum_fusion.2
  32.2 0.1 broadcast_in_dim_tile.7.sine_ref
  32.3 0.1 copy.13
  32.4 0.1 broadcast_in_dim_tile.6.cosine_ref
  32.6 0.1 copy.16.table_cosine_ref
  32.7 0.1 copy.17.table_sine_ref
  32.8 0.0 copy-start
  32.8 0.7 copy-done
  33.5 0.0 copy-start.1
  33.5 0.7 copy-done.1
  34.2 0.7 copy-done.2
  34.8 0.7 copy-done.3
  35.5 0.9 shard_map.105
  36.4 2.8 %collective-permute-start.4 = (bf16[128,512]{1,0:T(8,128)(2,1)S(1)}, bf16[128,512]{1,0:T(8,128)(2,1)S(1)}, u32[]{:S(2)}, u32[]{:S(2)}) collective-permute-start(bf16[128,512]{1,0:T(8,128)(2,1)S(1)} %collective-permute-done), channel_id=1, source_target_pairs={{0,16},{8,24},{16,0},{24,8},{32,48},{40,56},{48,32},{56,40},{64,80... | collective-permute-start | bytes 393224 | tf_op jit(solution)/shard_map/ppermute | solution.py:40
  39.2 2.8 %collective-permute-start.1 = (bf16[128,512]{1,0:T(8,128)(2,1)S(1)}, bf16[128,512]{1,0:T(8,128)(2,1)S(1)}, u32[]{:S(2)}, u32[]{:S(2)}) collective-permute-start(bf16[128,512]{1,0:T(8,128)(2,1)S(1)} %collective-permute-done), channel_id=1, source_target_pairs={{0,8},{8,16},{16,24},{24,0},{32,40},{40,48},{48,56},{56,32},{64,72... | collective-permute-start | bytes 393224 | tf_op jit(solution)/shard_map/ppermute | solution.py:40
  42.0 0.0 collective-permute-done.7
  42.0 1.2 fusion.17
  43.2 0.0 all-to-all-done
  43.2 0.0 copy-start.5
  43.2 3.2 %collective-permute-start.3 = (bf16[512,512]{1,0:T(8,128)(2,1)S(1)}, bf16[512,512]{1,0:T(8,128)(2,1)S(1)}, u32[]{:S(2)}, u32[]{:S(2)}) collective-permute-start(bf16[512,512]{1,0:T(8,128)(2,1)S(1)} %bitcast.58), channel_id=1, source_target_pairs={{0,480},{8,488},{16,496},{24,504},{32,0},{40,8},{48,16},{56,24},{6... | collective-permute-start | bytes 1572872 | tf_op jit(solution)/shard_map/ppermute | solution.py:21
  46.4 2.9 %collective-permute-start.2 = (bf16[512,512]{1,0:T(8,128)(2,1)S(1)}, bf16[512,512]{1,0:T(8,128)(2,1)S(1)}, u32[]{:S(2)}, u32[]{:S(2)}) collective-permute-start(bf16[512,512]{1,0:T(8,128)(2,1)S(1)} %bitcast.59), channel_id=1, source_target_pairs={{0,32},{8,40},{16,48},{24,56},{32,64},{40,72},{48,80},{56,88},{64,... | collective-permute-start | bytes 1572872 | tf_op jit(solution)/shard_map/ppermute | solution.py:21
  49.3 1.5 %fusion.15 = f32[512,512]{1,0:T(8,128)S(1)} fusion(bf16[512,512]{1,0:T(8,128)(2,1)S(1)} %bitcast.60, bf16[512,4096]{1,0:T(8,128)(2,1)} %bitcast.48, u32[]{:T(128)S(6)} %mul.106), kind=kOutput, calls=%fused_computation.20 | convolution fusion | flops 268435456 | bytes 2097156 | tf_op jit(solution)/shard_map/dot_general | solution.py:61
  50.8 1.2 convolution_add_fusion.4
  52.0 6.7 %collective-permute-done.3 = bf16[512,512]{1,0:T(8,128)(2,1)S(1)} collective-permute-done((bf16[512,512]{1,0:T(8,128)(2,1)S(1)}, bf16[512,512]{1,0:T(8,128)(2,1)S(1)}, u32[]{:S(2)}, u32[]{:S(2)}) %collective-permute-start.3) | collective-permute-done | bytes 524320 | tf_op jit(solution)/shard_map/ppermute | solution.py:21
  58.6 5.6 %collective-permute-start.6 = (bf16[512,512]{1,0:T(8,128)(2,1)S(1)}, bf16[512,512]{1,0:T(8,128)(2,1)S(1)}, u32[]{:S(2)}, u32[]{:S(2)}) collective-permute-start(bf16[512,512]{1,0:T(8,128)(2,1)S(1)} %collective-permute-done.3), channel_id=1, source_target_pairs={{0,480},{8,488},{16,496},{24,504},{32,0},{40,8},{48,16},{56,24},{6... | collective-permute-start | bytes 1572872 | tf_op jit(solution)/shard_map/ppermute | solution.py:21
  64.2 0.0 collective-permute-done.2
  64.2 1.9 %collective-permute-start.5 = (bf16[512,512]{1,0:T(8,128)(2,1)S(1)}, bf16[512,512]{1,0:T(8,128)(2,1)S(1)}, u32[]{:S(2)}, u32[]{:S(2)}) collective-permute-start(bf16[512,512]{1,0:T(8,128)(2,1)S(1)} %collective-permute-done.2), channel_id=1, source_target_pairs={{0,32},{8,40},{16,48},{24,56},{32,64},{40,72},{48,80},{56,88},{64,... | collective-permute-start | bytes 1572872 | tf_op jit(solution)/shard_map/ppermute | solution.py:21
  66.2 0.0 copy-done.5
  66.2 0.4 fusion.11
  66.6 0.4 fusion.13
  67.1 8.6 %collective-permute-done.6 = bf16[512,512]{1,0:T(8,128)(2,1)S(1)} collective-permute-done((bf16[512,512]{1,0:T(8,128)(2,1)S(1)}, bf16[512,512]{1,0:T(8,128)(2,1)S(1)}, u32[]{:S(2)}, u32[]{:S(2)}) %collective-permute-start.6) | collective-permute-done | bytes 524320 | tf_op jit(solution)/shard_map/ppermute | solution.py:21
  75.6 5.6 %collective-permute-start.9 = (bf16[512,512]{1,0:T(8,128)(2,1)S(1)}, bf16[512,512]{1,0:T(8,128)(2,1)S(1)}, u32[]{:S(2)}, u32[]{:S(2)}) collective-permute-start(bf16[512,512]{1,0:T(8,128)(2,1)S(1)} %collective-permute-done.6), channel_id=1, source_target_pairs={{0,480},{8,488},{16,496},{24,504},{32,0},{40,8},{48,16},{56,24},{6... | collective-permute-start | bytes 1572872 | tf_op jit(solution)/shard_map/ppermute | solution.py:21
  81.2 0.4 fusion.7
  81.7 0.0 collective-permute-done.5
  81.7 1.9 %collective-permute-start.8 = (bf16[512,512]{1,0:T(8,128)(2,1)S(1)}, bf16[512,512]{1,0:T(8,128)(2,1)S(1)}, u32[]{:S(2)}, u32[]{:S(2)}) collective-permute-start(bf16[512,512]{1,0:T(8,128)(2,1)S(1)} %collective-permute-done.5), channel_id=1, source_target_pairs={{0,32},{8,40},{16,48},{24,56},{32,64},{40,72},{48,80},{56,88},{64,... | collective-permute-start | bytes 1572872 | tf_op jit(solution)/shard_map/ppermute | solution.py:21
  83.6 0.4 fusion.9
  84.0 0.0 collective-permute-done.4
  84.0 0.3 fusion.4
  84.3 0.0 collective-permute-done.1
  84.3 0.3 fusion.3
  84.7 12.9 %collective-permute-done.8 = bf16[512,512]{1,0:T(8,128)(2,1)S(1)} collective-permute-done((bf16[512,512]{1,0:T(8,128)(2,1)S(1)}, bf16[512,512]{1,0:T(8,128)(2,1)S(1)}, u32[]{:S(2)}, u32[]{:S(2)}) %collective-permute-start.8) | collective-permute-done | bytes 524320 | tf_op jit(solution)/shard_map/ppermute | solution.py:21
  97.5 0.4 convolution_add_fusion.1
  98.0 0.0 copy-start.4
  98.0 0.0 collective-permute-done.9
  98.0 0.4 fusion.sums_ref
  98.4 0.7 shard_map.106
  99.1 18.9 %all_to_all.15 = bf16[32,8,384]{2,1,0:T(8,128)(2,1)S(1)} all-to-all(bf16[32,8,384]{2,1,0:T(8,128)(2,1)S(1)} %bitcast.42), channel_id=1, replica_groups=mesh['gr'=2,'sp'=32,'tp'=8] {'sp'}, dimensions={0} | all-to-all | bytes 393216 | tf_op jit(solution)/shard_map/all_to_all | solution.py:329
  118.1 0.6 shard_map.107
  118.7 20.8 %all_to_all.16 = bf16[32,8,384]{2,1,0:T(8,128)(2,1)S(1)} all-to-all(bf16[32,8,384]{2,1,0:T(8,128)(2,1)S(1)} %bitcast.44), channel_id=1, replica_groups=mesh['gr'=2,'sp'=32,'tp'=8] {'sp'}, dimensions={0} | all-to-all | bytes 393216 | tf_op jit(solution)/shard_map/all_to_all | solution.py:329
  139.4 0.0 copy-done.4
  139.4 1.3 shard_map.108
  (14 shorter events, 0.1 us)
Async XLA Ops:
  2.7 40.4 %all-to-all-start = ((bf16[4,128,512]{2,1,0:T(8,128)(2,1)}), bf16[4,128,512]{2,1,0:T(8,128)(2,1)S(1)}, u32[]{:S(2)}, u32[]{:S(2)}) async-start(bf16[4,128,512]{2,1,0:T(8,128)(2,1)} %get-tuple-element.16), calls=%async_computation | async-start | bytes 1048576 | tf_op jit(solution)/shard_map/all_to_all | solution.py:45
  7.2 19.8 %collective-permute-start = (bf16[128,512]{1,0:T(8,128)(2,1)}, bf16[128,512]{1,0:T(8,128)(2,1)S(1)}, u32[]{:S(2)}, u32[]{:S(2)}) collective-permute-start(bf16[128,512]{1,0:T(8,128)(2,1)} %get-tuple-element.17), channel_id=1, source_target_pairs={{0,384},{1,129},{2,386},{3,131},{4,388},{5,133},{6,390},{7,135},{8... | collective-permute-start | bytes 393224 | tf_op jit(solution)/shard_map/ppermute | solution.py:34
  26.9 15.0 %collective-permute-start.7 = (bf16[128,512]{1,0:T(8,128)(2,1)S(1)}, bf16[128,512]{1,0:T(8,128)(2,1)S(1)}, u32[]{:S(2)}, u32[]{:S(2)}) collective-permute-start(bf16[128,512]{1,0:T(8,128)(2,1)S(1)} %collective-permute-done), channel_id=1, source_target_pairs={{0,24},{8,0},{16,8},{24,16},{32,56},{40,32},{48,40},{56,48},{64,88... | collective-permute-start | bytes 393224 | tf_op jit(solution)/shard_map/ppermute | solution.py:40
  32.8 0.7 copy-start
  33.5 0.7 copy-start.1
  34.2 0.7 copy-start.2
  34.8 0.7 copy-start.3
  36.4 47.6 %collective-permute-start.4 = (bf16[128,512]{1,0:T(8,128)(2,1)S(1)}, bf16[128,512]{1,0:T(8,128)(2,1)S(1)}, u32[]{:S(2)}, u32[]{:S(2)}) collective-permute-start(bf16[128,512]{1,0:T(8,128)(2,1)S(1)} %collective-permute-done), channel_id=1, source_target_pairs={{0,16},{8,24},{16,0},{24,8},{32,48},{40,56},{48,32},{56,40},{64,80... | collective-permute-start | bytes 393224 | tf_op jit(solution)/shard_map/ppermute | solution.py:40
  39.2 45.1 %collective-permute-start.1 = (bf16[128,512]{1,0:T(8,128)(2,1)S(1)}, bf16[128,512]{1,0:T(8,128)(2,1)S(1)}, u32[]{:S(2)}, u32[]{:S(2)}) collective-permute-start(bf16[128,512]{1,0:T(8,128)(2,1)S(1)} %collective-permute-done), channel_id=1, source_target_pairs={{0,8},{8,16},{16,24},{24,0},{32,40},{40,48},{48,56},{56,32},{64,72... | collective-permute-start | bytes 393224 | tf_op jit(solution)/shard_map/ppermute | solution.py:40
  43.2 23.0 %copy-start.5 = (bf16[4,128,4096]{2,1,0:T(8,128)(2,1)S(1)}, bf16[4,128,4096]{2,1,0:T(8,128)(2,1)}, u32[]{:S(2)}) copy-start(bf16[4,128,4096]{2,1,0:T(8,128)(2,1)} %param.9) | copy-start | bytes 12582916
  43.2 15.5 %collective-permute-start.3 = (bf16[512,512]{1,0:T(8,128)(2,1)S(1)}, bf16[512,512]{1,0:T(8,128)(2,1)S(1)}, u32[]{:S(2)}, u32[]{:S(2)}) collective-permute-start(bf16[512,512]{1,0:T(8,128)(2,1)S(1)} %bitcast.58), channel_id=1, source_target_pairs={{0,480},{8,488},{16,496},{24,504},{32,0},{40,8},{48,16},{56,24},{6... | collective-permute-start | bytes 1572872 | tf_op jit(solution)/shard_map/ppermute | solution.py:21
  46.4 17.9 %collective-permute-start.2 = (bf16[512,512]{1,0:T(8,128)(2,1)S(1)}, bf16[512,512]{1,0:T(8,128)(2,1)S(1)}, u32[]{:S(2)}, u32[]{:S(2)}) collective-permute-start(bf16[512,512]{1,0:T(8,128)(2,1)S(1)} %bitcast.59), channel_id=1, source_target_pairs={{0,32},{8,40},{16,48},{24,56},{32,64},{40,72},{48,80},{56,88},{64,... | collective-permute-start | bytes 1572872 | tf_op jit(solution)/shard_map/ppermute | solution.py:21
  58.6 17.0 %collective-permute-start.6 = (bf16[512,512]{1,0:T(8,128)(2,1)S(1)}, bf16[512,512]{1,0:T(8,128)(2,1)S(1)}, u32[]{:S(2)}, u32[]{:S(2)}) collective-permute-start(bf16[512,512]{1,0:T(8,128)(2,1)S(1)} %collective-permute-done.3), channel_id=1, source_target_pairs={{0,480},{8,488},{16,496},{24,504},{32,0},{40,8},{48,16},{56,24},{6... | collective-permute-start | bytes 1572872 | tf_op jit(solution)/shard_map/ppermute | solution.py:21
  64.2 17.4 %collective-permute-start.5 = (bf16[512,512]{1,0:T(8,128)(2,1)S(1)}, bf16[512,512]{1,0:T(8,128)(2,1)S(1)}, u32[]{:S(2)}, u32[]{:S(2)}) collective-permute-start(bf16[512,512]{1,0:T(8,128)(2,1)S(1)} %collective-permute-done.2), channel_id=1, source_target_pairs={{0,32},{8,40},{16,48},{24,56},{32,64},{40,72},{48,80},{56,88},{64,... | collective-permute-start | bytes 1572872 | tf_op jit(solution)/shard_map/ppermute | solution.py:21
  75.6 22.4 %collective-permute-start.9 = (bf16[512,512]{1,0:T(8,128)(2,1)S(1)}, bf16[512,512]{1,0:T(8,128)(2,1)S(1)}, u32[]{:S(2)}, u32[]{:S(2)}) collective-permute-start(bf16[512,512]{1,0:T(8,128)(2,1)S(1)} %collective-permute-done.6), channel_id=1, source_target_pairs={{0,480},{8,488},{16,496},{24,504},{32,0},{40,8},{48,16},{56,24},{6... | collective-permute-start | bytes 1572872 | tf_op jit(solution)/shard_map/ppermute | solution.py:21
  81.7 15.9 %collective-permute-start.8 = (bf16[512,512]{1,0:T(8,128)(2,1)S(1)}, bf16[512,512]{1,0:T(8,128)(2,1)S(1)}, u32[]{:S(2)}, u32[]{:S(2)}) collective-permute-start(bf16[512,512]{1,0:T(8,128)(2,1)S(1)} %collective-permute-done.5), channel_id=1, source_target_pairs={{0,32},{8,40},{16,48},{24,56},{32,64},{40,72},{48,80},{56,88},{64,... | collective-permute-start | bytes 1572872 | tf_op jit(solution)/shard_map/ppermute | solution.py:21
  98.0 41.5 %copy-start.4 = (f32[256]{0:T(256)S(1)}, f32[256]{0:T(256)}, u32[]{:S(2)}) copy-start(f32[256]{0:T(256)} %param.17) | copy-start | bytes 3076

commit v3 on v2

--- a/solution.py
+++ b/solution.py
@@ -11,7 +11,6 @@
 Y = 4
 PARTS = 3
 EXTRA = 128
-EXACT = lax.Precision.HIGHEST
 F32, BF16 = (jnp.float32, jnp.bfloat16)
 
 
@@ -102,6 +101,16 @@
         copy.start()
     for copy in copies:
         copy.wait()
+
+
+def summed_where(x, chosen):
+    chosen, total = (chosen.astype(BF16), None)
+    for _ in range(PARTS):
+        part = x.astype(BF16)
+        product = jnp.dot(part, chosen, preferred_element_type=F32)
+        total = product if total is None else total + product
+        x = x - part.astype(F32)
+    return total
 
 
 def share_kernel(seqs, sums_ref, cosine_ref, sine_ref, carried_ref, out_ref):
@@ -155,7 +164,7 @@
     spread = (rows_of((cols // HEAD_DIM, cols)) == lanes_of((cols // HEAD_DIM, cols)) // HEAD_DIM)
     for seq in range(seqs):
         there = pl.ds(seq * span, span)
-        weight = jnp.dot(weight_ref[there, :], spread.astype(F32), precision=EXACT)
+        weight = summed_where(weight_ref[there, :], spread)
         faded_cosine_ref[there, :] = table_cosine_ref[...] * weight
         faded_sine_ref[there, :] = table_sine_ref[...] * weight
     heads, lanes = (cols // HEAD_DIM, seqs * HEAD_DIM)
@@ -173,10 +182,10 @@
         u = ref[...].astype(F32)
         other = jnp.where(low, pltpu.roll(u, cols - half, 1), pltpu.roll(u, half, 1))
         turned = u * cosine_ref[...] + other * sine_ref[...]
-        picked = jnp.dot(turned, pick.astype(F32), precision=EXACT)
+        picked = summed_where(turned, pick)
         return jnp.sum(jnp.where(own, picked, 0.0), axis=0, keepdims=True)
 
-    decay = jnp.dot(jnp.exp(decay_ref[...]), own.astype(F32), precision=EXACT)
+    decay = summed_where(jnp.exp(decay_ref[...]), own)
     here = rows_of((heads, lanes)) == head
     lines_ref[0:1] = jnp.sum(jnp.where(here, decay, 0.0), axis=0, keepdims=True)
     lines_ref[1:2] = line(key_ref) * HEAD_DIM ** (-0.5)
@@ -185,7 +194,7 @@
     values = lax.dot_general(
         spot.astype(BF16), value_ref[...], (((1,), (1,)), ((), ())), preferred_element_type=F32
     )
-    values_ref[...] = jnp.dot(values, own.astype(F32), precision=EXACT)
+    values_ref[...] = summed_where(values, own)
 
 
 def owner_kernel(devices, seqs, got_ref, lines_ref, values_ref, out_ref):
@@ -196,8 +205,8 @@
     )
     sums = jnp.dot(later.astype(BF16), got_ref[:, lanes:], preferred_element_type=F32)
     place = (EXTRA, lanes)
-    wide = (rows_of(place) // PARTS == lanes_of(place) // HEAD_DIM).astype(F32)
-    fade = jnp.exp(jnp.dot(sums, wide, precision=EXACT))
+    wide = rows_of(place) // PARTS == lanes_of(place) // HEAD_DIM
+    fade = jnp.exp(summed_where(sums, wide))
     shares = got_ref[:, :lanes].astype(F32)
     owned = shares[:rows] * fade[0:1]
     for device in range(1, devices):
@@ -205,7 +214,7 @@
     finished = lines_ref[0:1] * owned + lines_ref[1:2] * values_ref[...]
     place = (lanes, EXTRA)
     fold = rows_of(place) // HEAD_DIM == lanes_of(place) % seqs
-    read = jnp.dot(finished * lines_ref[2:3], fold.astype(F32), precision=EXACT)
+    read = summed_where(finished * lines_ref[2:3], fold)
     piece = lanes_of(read.shape) // seqs
     rest, packed = (read, jnp.zeros_like(read))
     for part in range(PARTS):
@@ -225,9 +234,9 @@
         pick.astype(BF16), got_ref[:, lanes:], (((1,), (1,)), ((), ())), preferred_element_type=F32
     )
     place = (cols, cols)
-    mean = (rows_of(place) // HEAD_DIM == lanes_of(place) // HEAD_DIM).astype(F32) / HEAD_DIM
-    center = raw - jnp.dot(raw, mean, precision=EXACT)
-    spread = jnp.dot(center * center, mean, precision=EXACT)
+    head = rows_of(place) // HEAD_DIM == lanes_of(place) // HEAD_DIM
+    center = raw - summed_where(raw, head) / HEAD_DIM
+    spread = summed_where(center * center, head) / HEAD_DIM
     normed = center * lax.rsqrt(spread + 1e-06) * gain_ref[...]
     read_ref[...] = normed[:seqs].astype(BF16)
 

time: 142 us -> 141 us (level)
  the two profiles are of different devices: /device:TPU:2 before, /device:TPU:4 now
where the time goes in v3:
time: 141 us; the launch traced here: 140 us
  starting transfers between devices  49 us (35%)
  blocking collectives  39.7 us (28%)
  waiting for transfers between devices  31.5 us (22%)
  matrix products  7.09 us (5%)
  Pallas kernels  4.95 us (4%)
  local copies, waits for them, and re-layouts  3.51 us (2%)
  other arithmetic  3.49 us (2%)
    all_to_all x2, blocking collectives, exchanged(): return lax.all_to_all(cut, 'sp', 0, 0, tiled=True).reshape(x.shape)  39.7 us
    ppermute x6, waiting for transfers between devices, moved_along_z(): return lax.ppermute(x, ('gr', 'sp'), pairs)  28.1 us
    ppermute x6, starting transfers between devices, moved_along_z(): return lax.ppermute(x, ('gr', 'sp'), pairs)  21.1 us
    ppermute x1, starting transfers between devices, from_opposite_plane(): return lax.ppermute(x, ('gr', 'sp', 'tp'), pairs)  12.7 us
    ppermute x3, starting transfers between devices, moved_along_y(): return lax.ppermute(x, 'sp', pairs)  10.7 us
    dot_general x11, matrix products, part(): return jnp.dot(cols, weights, preferred_element_type=F32)  7.09 us
    all_to_all x1, starting transfers between devices, exchanged_along_y(): lax.all_to_all(spread, 'sp', 0, 0, tiled=True, axis_index_groups=groups)  4.48 us
    ppermute x1, waiting for transfers between devices, from_opposite_plane(): return lax.ppermute(x, ('gr', 'sp', 'tp'), pairs)  3.36 us
  transfers between devices with their start and end apart: 11, of which 4 were waited for; matrix products, arithmetic and copies ran while one was open for 8% of the time, Pallas kernels for 0%

profile of v3, /device:TPU:4, one launch (start us, length us, event | category | flops | bytes accessed | tf_op | source)
XLA Modules:
  0.0 140.1 jit_solution(12764623933437984038)
XLA Ops:
  0.6 2.1 %shard_map.104 = (bf16[128,512]{1,0:T(8,128)(2,1)}, bf16[4,128,512]{2,1,0:T(8,128)(2,1)}) custom-call(bf16[128,256]{1,0:T(8,128)(2,1)} %key_ref.2, bf16[128,256]{1,0:T(8,128)(2,1)} %value_ref.2), custom_call_target="tpu_custom_call" | custom-call | tf_op jit(solution)/shard_map/pallas_call | solution.py:298
  2.7 4.5 %all-to-all-start = ((bf16[4,128,512]{2,1,0:T(8,128)(2,1)}), bf16[4,128,512]{2,1,0:T(8,128)(2,1)S(1)}, u32[]{:S(2)}, u32[]{:S(2)}) async-start(bf16[4,128,512]{2,1,0:T(8,128)(2,1)} %get-tuple-element.16), calls=%async_computation | async-start | bytes 1048576 | tf_op jit(solution)/shard_map/all_to_all | solution.py:44
  7.2 12.7 %collective-permute-start = (bf16[128,512]{1,0:T(8,128)(2,1)}, bf16[128,512]{1,0:T(8,128)(2,1)S(1)}, u32[]{:S(2)}, u32[]{:S(2)}) collective-permute-start(bf16[128,512]{1,0:T(8,128)(2,1)} %get-tuple-element.17), channel_id=1, source_target_pairs={{0,384},{1,129},{2,386},{3,131},{4,388},{5,133},{6,390},{7,135},{8... | collective-permute-start | bytes 393224 | tf_op jit(solution)/shard_map/ppermute | solution.py:33
  19.9 0.1 multiply_sine_fusion.1
  20.0 0.8 reduce_sum.11
  20.8 2.3 %reduce_window_sum.13 = f32[4,4,128]{2,1,0:T(4,128)S(1)} reduce-window(f32[4,4,128]{2,1,0:T(4,128)} %param.12, f32[]{:T(128)} %constant.121.clone.1), window={size=1x1x128 pad=0_0x0_0x127_0}, to_apply=%region_1.0 | reduce-window | flops 260096 | bytes 16388 | tf_op jit(solution)/shard_map/jit(cumsum)/reduce_window_sum | solution.py:282
  23.1 0.1 copy.14
  23.2 0.1 broadcast_in_dim.16
  23.3 0.1 fusion.25
  23.4 0.1 fusion.24
  23.5 0.1 multiply_cosine_fusion.1
  23.6 3.4 %collective-permute-done = bf16[128,512]{1,0:T(8,128)(2,1)S(1)} collective-permute-done((bf16[128,512]{1,0:T(8,128)(2,1)}, bf16[128,512]{1,0:T(8,128)(2,1)S(1)}, u32[]{:S(2)}, u32[]{:S(2)}) %collective-permute-start) | collective-permute-done | bytes 131104 | tf_op jit(solution)/shard_map/ppermute | solution.py:33
  26.9 5.1 %collective-permute-start.7 = (bf16[128,512]{1,0:T(8,128)(2,1)S(1)}, bf16[128,512]{1,0:T(8,128)(2,1)S(1)}, u32[]{:S(2)}, u32[]{:S(2)}) collective-permute-start(bf16[128,512]{1,0:T(8,128)(2,1)S(1)} %collective-permute-done), channel_id=1, source_target_pairs={{0,24},{8,0},{16,8},{24,16},{32,56},{40,32},{48,40},{56,48},{64,88... | collective-permute-start | bytes 393224 | tf_op jit(solution)/shard_map/ppermute | solution.py:39
  32.1 0.1 pad_maximum_fusion.2
  32.2 0.1 broadcast_in_dim_tile.7.sine_ref
  32.3 0.1 copy.13
  32.4 0.1 broadcast_in_dim_tile.6.cosine_ref
  32.6 0.1 copy.16.table_cosine_ref
  32.7 0.1 copy.17.table_sine_ref
  32.8 0.0 copy-start
  32.8 0.7 copy-done
  33.5 0.7 copy-done.1
  34.2 0.0 copy-start.2
  34.2 0.7 copy-done.2
  34.8 0.7 copy-done.3
  35.5 0.6 shard_map.105
  36.1 2.8 %collective-permute-start.4 = (bf16[128,512]{1,0:T(8,128)(2,1)S(1)}, bf16[128,512]{1,0:T(8,128)(2,1)S(1)}, u32[]{:S(2)}, u32[]{:S(2)}) collective-permute-start(bf16[128,512]{1,0:T(8,128)(2,1)S(1)} %collective-permute-done), channel_id=1, source_target_pairs={{0,16},{8,24},{16,0},{24,8},{32,48},{40,56},{48,32},{56,40},{64,80... | collective-permute-start | bytes 393224 | tf_op jit(solution)/shard_map/ppermute | solution.py:39
  38.9 2.8 %collective-permute-start.1 = (bf16[128,512]{1,0:T(8,128)(2,1)S(1)}, bf16[128,512]{1,0:T(8,128)(2,1)S(1)}, u32[]{:S(2)}, u32[]{:S(2)}) collective-permute-start(bf16[128,512]{1,0:T(8,128)(2,1)S(1)} %collective-permute-done), channel_id=1, source_target_pairs={{0,8},{8,16},{16,24},{24,0},{32,40},{40,48},{48,56},{56,32},{64,72... | collective-permute-start | bytes 393224 | tf_op jit(solution)/shard_map/ppermute | solution.py:39
  41.6 0.0 collective-permute-done.7
  41.6 1.2 fusion.17
  42.8 0.0 all-to-all-done
  42.8 0.0 copy-start.5
  42.9 3.2 %collective-permute-start.3 = (bf16[512,512]{1,0:T(8,128)(2,1)S(1)}, bf16[512,512]{1,0:T(8,128)(2,1)S(1)}, u32[]{:S(2)}, u32[]{:S(2)}) collective-permute-start(bf16[512,512]{1,0:T(8,128)(2,1)S(1)} %bitcast.58), channel_id=1, source_target_pairs={{0,480},{8,488},{16,496},{24,504},{32,0},{40,8},{48,16},{56,24},{6... | collective-permute-start | bytes 1572872 | tf_op jit(solution)/shard_map/ppermute | solution.py:20
  46.0 2.9 %collective-permute-start.2 = (bf16[512,512]{1,0:T(8,128)(2,1)S(1)}, bf16[512,512]{1,0:T(8,128)(2,1)S(1)}, u32[]{:S(2)}, u32[]{:S(2)}) collective-permute-start(bf16[512,512]{1,0:T(8,128)(2,1)S(1)} %bitcast.59), channel_id=1, source_target_pairs={{0,32},{8,40},{16,48},{24,56},{32,64},{40,72},{48,80},{56,88},{64,... | collective-permute-start | bytes 1572872 | tf_op jit(solution)/shard_map/ppermute | solution.py:20
  49.0 1.5 %fusion.15 = f32[512,512]{1,0:T(8,128)S(1)} fusion(bf16[512,512]{1,0:T(8,128)(2,1)S(1)} %bitcast.60, bf16[512,4096]{1,0:T(8,128)(2,1)} %bitcast.48, u32[]{:T(128)S(6)} %mul.106), kind=kOutput, calls=%fused_computation.20 | convolution fusion | flops 268435456 | bytes 2097156 | tf_op jit(solution)/shard_map/dot_general | solution.py:60
  50.5 1.2 convolution_add_fusion.4
  51.7 6.7 %collective-permute-done.3 = bf16[512,512]{1,0:T(8,128)(2,1)S(1)} collective-permute-done((bf16[512,512]{1,0:T(8,128)(2,1)S(1)}, bf16[512,512]{1,0:T(8,128)(2,1)S(1)}, u32[]{:S(2)}, u32[]{:S(2)}) %collective-permute-start.3) | collective-permute-done | bytes 524320 | tf_op jit(solution)/shard_map/ppermute | solution.py:20
  58.3 5.6 %collective-permute-start.6 = (bf16[512,512]{1,0:T(8,128)(2,1)S(1)}, bf16[512,512]{1,0:T(8,128)(2,1)S(1)}, u32[]{:S(2)}, u32[]{:S(2)}) collective-permute-start(bf16[512,512]{1,0:T(8,128)(2,1)S(1)} %collective-permute-done.3), channel_id=1, source_target_pairs={{0,480},{8,488},{16,496},{24,504},{32,0},{40,8},{48,16},{56,24},{6... | collective-permute-start | bytes 1572872 | tf_op jit(solution)/shard_map/ppermute | solution.py:20
  63.9 0.0 collective-permute-done.2
  63.9 1.9 %collective-permute-start.5 = (bf16[512,512]{1,0:T(8,128)(2,1)S(1)}, bf16[512,512]{1,0:T(8,128)(2,1)S(1)}, u32[]{:S(2)}, u32[]{:S(2)}) collective-permute-start(bf16[512,512]{1,0:T(8,128)(2,1)S(1)} %collective-permute-done.2), channel_id=1, source_target_pairs={{0,32},{8,40},{16,48},{24,56},{32,64},{40,72},{48,80},{56,88},{64,... | collective-permute-start | bytes 1572872 | tf_op jit(solution)/shard_map/ppermute | solution.py:20
  65.8 0.0 copy-done.5
  65.9 0.4 fusion.11
  66.3 0.4 fusion.13
  66.7 8.6 %collective-permute-done.6 = bf16[512,512]{1,0:T(8,128)(2,1)S(1)} collective-permute-done((bf16[512,512]{1,0:T(8,128)(2,1)S(1)}, bf16[512,512]{1,0:T(8,128)(2,1)S(1)}, u32[]{:S(2)}, u32[]{:S(2)}) %collective-permute-start.6) | collective-permute-done | bytes 524320 | tf_op jit(solution)/shard_map/ppermute | solution.py:20
  75.3 5.6 %collective-permute-start.9 = (bf16[512,512]{1,0:T(8,128)(2,1)S(1)}, bf16[512,512]{1,0:T(8,128)(2,1)S(1)}, u32[]{:S(2)}, u32[]{:S(2)}) collective-permute-start(bf16[512,512]{1,0:T(8,128)(2,1)S(1)} %collective-permute-done.6), channel_id=1, source_target_pairs={{0,480},{8,488},{16,496},{24,504},{32,0},{40,8},{48,16},{56,24},{6... | collective-permute-start | bytes 1572872 | tf_op jit(solution)/shard_map/ppermute | solution.py:20
  80.9 0.4 fusion.7
  81.3 0.0 collective-permute-done.5
  81.4 1.9 %collective-permute-start.8 = (bf16[512,512]{1,0:T(8,128)(2,1)S(1)}, bf16[512,512]{1,0:T(8,128)(2,1)S(1)}, u32[]{:S(2)}, u32[]{:S(2)}) collective-permute-start(bf16[512,512]{1,0:T(8,128)(2,1)S(1)} %collective-permute-done.5), channel_id=1, source_target_pairs={{0,32},{8,40},{16,48},{24,56},{32,64},{40,72},{48,80},{56,88},{64,... | collective-permute-start | bytes 1572872 | tf_op jit(solution)/shard_map/ppermute | solution.py:20
  83.3 0.4 fusion.9
  83.7 0.0 collective-permute-done.4
  83.7 0.3 fusion.4
  84.0 0.0 collective-permute-done.1
  84.0 0.3 fusion.3
  84.4 12.9 %collective-permute-done.8 = bf16[512,512]{1,0:T(8,128)(2,1)S(1)} collective-permute-done((bf16[512,512]{1,0:T(8,128)(2,1)S(1)}, bf16[512,512]{1,0:T(8,128)(2,1)S(1)}, u32[]{:S(2)}, u32[]{:S(2)}) %collective-permute-start.8) | collective-permute-done | bytes 524320 | tf_op jit(solution)/shard_map/ppermute | solution.py:20
  97.2 0.4 convolution_add_fusion.1
  97.7 0.0 copy-start.4
  97.7 0.0 collective-permute-done.9
  97.7 0.4 fusion.sums_ref
  98.2 0.7 shard_map.106
  98.8 18.9 %all_to_all.15 = bf16[32,8,384]{2,1,0:T(8,128)(2,1)S(1)} all-to-all(bf16[32,8,384]{2,1,0:T(8,128)(2,1)S(1)} %bitcast.42), channel_id=1, replica_groups=mesh['gr'=2,'sp'=32,'tp'=8] {'sp'}, dimensions={0} | all-to-all | bytes 393216 | tf_op jit(solution)/shard_map/all_to_all | solution.py:338
  117.7 0.5 shard_map.107
  118.2 20.8 %all_to_all.16 = bf16[32,8,384]{2,1,0:T(8,128)(2,1)S(1)} all-to-all(bf16[32,8,384]{2,1,0:T(8,128)(2,1)S(1)} %bitcast.44), channel_id=1, replica_groups=mesh['gr'=2,'sp'=32,'tp'=8] {'sp'}, dimensions={0} | all-to-all | bytes 393216 | tf_op jit(solution)/shard_map/all_to_all | solution.py:338
  139.0 0.0 copy-done.4
  139.0 1.1 shard_map.108
  (14 shorter events, 0.1 us)
Async XLA Ops:
  2.7 40.1 %all-to-all-start = ((bf16[4,128,512]{2,1,0:T(8,128)(2,1)}), bf16[4,128,512]{2,1,0:T(8,128)(2,1)S(1)}, u32[]{:S(2)}, u32[]{:S(2)}) async-start(bf16[4,128,512]{2,1,0:T(8,128)(2,1)} %get-tuple-element.16), calls=%async_computation | async-start | bytes 1048576 | tf_op jit(solution)/shard_map/all_to_all | solution.py:44
  7.2 19.8 %collective-permute-start = (bf16[128,512]{1,0:T(8,128)(2,1)}, bf16[128,512]{1,0:T(8,128)(2,1)S(1)}, u32[]{:S(2)}, u32[]{:S(2)}) collective-permute-start(bf16[128,512]{1,0:T(8,128)(2,1)} %get-tuple-element.17), channel_id=1, source_target_pairs={{0,384},{1,129},{2,386},{3,131},{4,388},{5,133},{6,390},{7,135},{8... | collective-permute-start | bytes 393224 | tf_op jit(solution)/shard_map/ppermute | solution.py:33
  26.9 14.7 %collective-permute-start.7 = (bf16[128,512]{1,0:T(8,128)(2,1)S(1)}, bf16[128,512]{1,0:T(8,128)(2,1)S(1)}, u32[]{:S(2)}, u32[]{:S(2)}) collective-permute-start(bf16[128,512]{1,0:T(8,128)(2,1)S(1)} %collective-permute-done), channel_id=1, source_target_pairs={{0,24},{8,0},{16,8},{24,16},{32,56},{40,32},{48,40},{56,48},{64,88... | collective-permute-start | bytes 393224 | tf_op jit(solution)/shard_map/ppermute | solution.py:39
  32.8 0.7 copy-start
  33.5 0.7 copy-start.1
  34.2 0.7 copy-start.2
  34.8 0.7 copy-start.3
  36.1 47.6 %collective-permute-start.4 = (bf16[128,512]{1,0:T(8,128)(2,1)S(1)}, bf16[128,512]{1,0:T(8,128)(2,1)S(1)}, u32[]{:S(2)}, u32[]{:S(2)}) collective-permute-start(bf16[128,512]{1,0:T(8,128)(2,1)S(1)} %collective-permute-done), channel_id=1, source_target_pairs={{0,16},{8,24},{16,0},{24,8},{32,48},{40,56},{48,32},{56,40},{64,80... | collective-permute-start | bytes 393224 | tf_op jit(solution)/shard_map/ppermute | solution.py:39
  38.9 45.2 %collective-permute-start.1 = (bf16[128,512]{1,0:T(8,128)(2,1)S(1)}, bf16[128,512]{1,0:T(8,128)(2,1)S(1)}, u32[]{:S(2)}, u32[]{:S(2)}) collective-permute-start(bf16[128,512]{1,0:T(8,128)(2,1)S(1)} %collective-permute-done), channel_id=1, source_target_pairs={{0,8},{8,16},{16,24},{24,0},{32,40},{40,48},{48,56},{56,32},{64,72... | collective-permute-start | bytes 393224 | tf_op jit(solution)/shard_map/ppermute | solution.py:39
  42.8 23.0 %copy-start.5 = (bf16[4,128,4096]{2,1,0:T(8,128)(2,1)S(1)}, bf16[4,128,4096]{2,1,0:T(8,128)(2,1)}, u32[]{:S(2)}) copy-start(bf16[4,128,4096]{2,1,0:T(8,128)(2,1)} %param.9) | copy-start | bytes 12582916
  42.9 15.5 %collective-permute-start.3 = (bf16[512,512]{1,0:T(8,128)(2,1)S(1)}, bf16[512,512]{1,0:T(8,128)(2,1)S(1)}, u32[]{:S(2)}, u32[]{:S(2)}) collective-permute-start(bf16[512,512]{1,0:T(8,128)(2,1)S(1)} %bitcast.58), channel_id=1, source_target_pairs={{0,480},{8,488},{16,496},{24,504},{32,0},{40,8},{48,16},{56,24},{6... | collective-permute-start | bytes 1572872 | tf_op jit(solution)/shard_map/ppermute | solution.py:20
  46.0 17.9 %collective-permute-start.2 = (bf16[512,512]{1,0:T(8,128)(2,1)S(1)}, bf16[512,512]{1,0:T(8,128)(2,1)S(1)}, u32[]{:S(2)}, u32[]{:S(2)}) collective-permute-start(bf16[512,512]{1,0:T(8,128)(2,1)S(1)} %bitcast.59), channel_id=1, source_target_pairs={{0,32},{8,40},{16,48},{24,56},{32,64},{40,72},{48,80},{56,88},{64,... | collective-permute-start | bytes 1572872 | tf_op jit(solution)/shard_map/ppermute | solution.py:20
  58.3 17.0 %collective-permute-start.6 = (bf16[512,512]{1,0:T(8,128)(2,1)S(1)}, bf16[512,512]{1,0:T(8,128)(2,1)S(1)}, u32[]{:S(2)}, u32[]{:S(2)}) collective-permute-start(bf16[512,512]{1,0:T(8,128)(2,1)S(1)} %collective-permute-done.3), channel_id=1, source_target_pairs={{0,480},{8,488},{16,496},{24,504},{32,0},{40,8},{48,16},{56,24},{6... | collective-permute-start | bytes 1572872 | tf_op jit(solution)/shard_map/ppermute | solution.py:20
  63.9 17.4 %collective-permute-start.5 = (bf16[512,512]{1,0:T(8,128)(2,1)S(1)}, bf16[512,512]{1,0:T(8,128)(2,1)S(1)}, u32[]{:S(2)}, u32[]{:S(2)}) collective-permute-start(bf16[512,512]{1,0:T(8,128)(2,1)S(1)} %collective-permute-done.2), channel_id=1, source_target_pairs={{0,32},{8,40},{16,48},{24,56},{32,64},{40,72},{48,80},{56,88},{64,... | collective-permute-start | bytes 1572872 | tf_op jit(solution)/shard_map/ppermute | solution.py:20
  75.3 22.4 %collective-permute-start.9 = (bf16[512,512]{1,0:T(8,128)(2,1)S(1)}, bf16[512,512]{1,0:T(8,128)(2,1)S(1)}, u32[]{:S(2)}, u32[]{:S(2)}) collective-permute-start(bf16[512,512]{1,0:T(8,128)(2,1)S(1)} %collective-permute-done.6), channel_id=1, source_target_pairs={{0,480},{8,488},{16,496},{24,504},{32,0},{40,8},{48,16},{56,24},{6... | collective-permute-start | bytes 1572872 | tf_op jit(solution)/shard_map/ppermute | solution.py:20
  81.4 15.9 %collective-permute-start.8 = (bf16[512,512]{1,0:T(8,128)(2,1)S(1)}, bf16[512,512]{1,0:T(8,128)(2,1)S(1)}, u32[]{:S(2)}, u32[]{:S(2)}) collective-permute-start(bf16[512,512]{1,0:T(8,128)(2,1)S(1)} %collective-permute-done.5), channel_id=1, source_target_pairs={{0,32},{8,40},{16,48},{24,56},{32,64},{40,72},{48,80},{56,88},{64,... | collective-permute-start | bytes 1572872 | tf_op jit(solution)/shard_map/ppermute | solution.py:20
  97.7 41.3 %copy-start.4 = (f32[256]{0:T(256)S(1)}, f32[256]{0:T(256)}, u32[]{:S(2)}) copy-start(f32[256]{0:T(256)} %param.17) | copy-start | bytes 3076

commit v4 on v3

--- a/solution.py
+++ b/solution.py
@@ -91,12 +91,20 @@
     return lax.broadcasted_iota(jnp.int32, shape, 0)
 
 
-def spread_kernel(key_ref, value_ref, own_ref, spread_ref, sems):
+def spread_kernel(key_ref, value_ref, own_ref, spread_ref, both_ref, in_sems, out_sems):
     cols = key_ref.shape[1]
-    copies = []
-    for ref, cut in ((key_ref, pl.ds(0, cols)), (value_ref, pl.ds(cols, cols))):
-        for to in (own_ref.at[:, cut], *(spread_ref.at[y, :, cut] for y in range(Y))):
-            copies.append(pltpu.make_async_copy(ref, to, sems.at[len(copies)]))
+    loads = [
+        pltpu.make_async_copy(ref, both_ref.at[:, pl.ds(n * cols, cols)], in_sems.at[n])
+        for n, ref in enumerate((key_ref, value_ref))
+    ]
+    for load in loads:
+        load.start()
+    for load in loads:
+        load.wait()
+    places = (*(spread_ref.at[y] for y in range(Y)), own_ref)
+    copies = [
+        pltpu.make_async_copy(both_ref, to, out_sems.at[n]) for n, to in enumerate(places)
+    ]
     for copy in copies:
         copy.start()
     for copy in copies:
@@ -279,7 +287,8 @@
     sine = jnp.sin(angles) * HEAD_DIM ** (-0.5)
     sine = jnp.tile(jnp.concatenate([-sine, sine], axis=1), (1, heads))
     totals = jnp.sum(log_decay, axis=-1)
-    weight = jnp.exp(totals[:, :, None] - jnp.cumsum(log_decay, axis=-1))
+    summed = jnp.cumsum(log_decay, axis=-1)
+    weight = jnp.exp(totals[:, :, None] - summed)
     weight = jnp.transpose(weight, (1, 2, 0)).reshape(seqs * span, heads)
     carried = jnp.stack(in_three(totals), axis=-1).reshape(heads, 1, 1, seqs * PARTS)
     carried = jnp.broadcast_to(carried, (heads, devices // heads, 1, seqs * PARTS))
@@ -302,8 +311,12 @@
             jax.ShapeDtypeStruct((Y, depth, 2 * cols), BF16),
         ],
         in_specs=[pl.BlockSpec(memory_space=pl.ANY)] * 2,
-        out_specs=[pl.BlockSpec(memory_space=pltpu.VMEM)] * 2,
-        scratch_shapes=[pltpu.SemaphoreType.DMA((2 * (Y + 1),))],
+        out_specs=[pl.BlockSpec(memory_space=pl.ANY)] * 2,
+        scratch_shapes=[
+            pltpu.VMEM((depth, 2 * cols), BF16),
+            pltpu.SemaphoreType.DMA((2,)),
+            pltpu.SemaphoreType.DMA((Y + 1,)),
+        ],
     )(key_weight, value_weight)
     sums = projected(tokens.reshape(seqs * span, width), own, spread)
     place = pl.BlockSpec(memory_space=pltpu.SMEM)

time: 141 us -> 141 us (level)
  the two profiles are of different devices: /device:TPU:4 before, /device:TPU:2 now
where the time goes in v4:
time: 141 us; the launch traced here: 140 us
  starting transfers between devices  48.9 us (35%)
  blocking collectives  39.7 us (28%)
  waiting for transfers between devices  31.5 us (22%)
  matrix products  7.09 us (5%)
  Pallas kernels  4.62 us (3%)
  local copies, waits for them, and re-layouts  3.51 us (2%)
  other arithmetic  3.49 us (2%)
    all_to_all x2, blocking collectives, exchanged(): return lax.all_to_all(cut, 'sp', 0, 0, tiled=True).reshape(x.shape)  39.7 us
    ppermute x6, waiting for transfers between devices, moved_along_z(): return lax.ppermute(x, ('gr', 'sp'), pairs)  28.1 us
    ppermute x6, starting transfers between devices, moved_along_z(): return lax.ppermute(x, ('gr', 'sp'), pairs)  21.1 us
    ppermute x1, starting transfers between devices, from_opposite_plane(): return lax.ppermute(x, ('gr', 'sp', 'tp'), pairs)  12.7 us
    ppermute x3, starting transfers between devices, moved_along_y(): return lax.ppermute(x, 'sp', pairs)  10.7 us
    dot_general x11, matrix products, part(): return jnp.dot(cols, weights, preferred_element_type=F32)  7.09 us
    all_to_all x1, starting transfers between devices, exchanged_along_y(): lax.all_to_all(spread, 'sp', 0, 0, tiled=True, axis_index_groups=groups)  4.48 us
    ppermute x1, waiting for transfers between devices, from_opposite_plane(): return lax.ppermute(x, ('gr', 'sp', 'tp'), pairs)  3.36 us
  transfers between devices with their start and end apart: 11, of which 4 were waited for; matrix products, arithmetic and copies ran while one was open for 8% of the time, Pallas kernels for 0%

profile of v4, /device:TPU:2, one launch (start us, length us, event | category | flops | bytes accessed | tf_op | source)
XLA Modules:
  0.0 139.8 jit_solution(10853418640247190474)
XLA Ops:
  0.6 1.8 %shard_map.104 = (bf16[128,512]{1,0:T(8,128)(2,1)}, bf16[4,128,512]{2,1,0:T(8,128)(2,1)}) custom-call(bf16[128,256]{1,0:T(8,128)(2,1)} %key_ref.2, bf16[128,256]{1,0:T(8,128)(2,1)} %value_ref.2), custom_call_target="tpu_custom_call" | custom-call | tf_op jit(solution)/shard_map/pallas_call | solution.py:307
  2.4 4.5 %all-to-all-start = ((bf16[4,128,512]{2,1,0:T(8,128)(2,1)}), bf16[4,128,512]{2,1,0:T(8,128)(2,1)S(1)}, u32[]{:S(2)}, u32[]{:S(2)}) async-start(bf16[4,128,512]{2,1,0:T(8,128)(2,1)} %get-tuple-element.16), calls=%async_computation | async-start | bytes 1048576 | tf_op jit(solution)/shard_map/all_to_all | solution.py:44
  6.9 12.7 %collective-permute-start = (bf16[128,512]{1,0:T(8,128)(2,1)}, bf16[128,512]{1,0:T(8,128)(2,1)S(1)}, u32[]{:S(2)}, u32[]{:S(2)}) collective-permute-start(bf16[128,512]{1,0:T(8,128)(2,1)} %get-tuple-element.17), channel_id=1, source_target_pairs={{0,384},{1,129},{2,386},{3,131},{4,388},{5,133},{6,390},{7,135},{8... | collective-permute-start | bytes 393224 | tf_op jit(solution)/shard_map/ppermute | solution.py:33
  19.6 0.1 multiply_sine_fusion.1
  19.7 0.8 reduce_sum.11
  20.5 2.3 %reduce_window_sum.13 = f32[4,4,128]{2,1,0:T(4,128)S(1)} reduce-window(f32[4,4,128]{2,1,0:T(4,128)} %param.12, f32[]{:T(128)} %constant.121.clone.1), window={size=1x1x128 pad=0_0x0_0x127_0}, to_apply=%region_1.0 | reduce-window | flops 260096 | bytes 16388 | tf_op jit(solution)/shard_map/jit(cumsum)/reduce_window_sum | solution.py:290
  22.7 0.1 copy.14
  22.9 0.1 broadcast_in_dim.16
  23.0 0.1 fusion.25
  23.1 0.1 fusion.24
  23.2 0.1 multiply_cosine_fusion.1
  23.3 3.4 %collective-permute-done = bf16[128,512]{1,0:T(8,128)(2,1)S(1)} collective-permute-done((bf16[128,512]{1,0:T(8,128)(2,1)}, bf16[128,512]{1,0:T(8,128)(2,1)S(1)}, u32[]{:S(2)}, u32[]{:S(2)}) %collective-permute-start) | collective-permute-done | bytes 131104 | tf_op jit(solution)/shard_map/ppermute | solution.py:33
  26.6 5.1 %collective-permute-start.7 = (bf16[128,512]{1,0:T(8,128)(2,1)S(1)}, bf16[128,512]{1,0:T(8,128)(2,1)S(1)}, u32[]{:S(2)}, u32[]{:S(2)}) collective-permute-start(bf16[128,512]{1,0:T(8,128)(2,1)S(1)} %collective-permute-done), channel_id=1, source_target_pairs={{0,24},{8,0},{16,8},{24,16},{32,56},{40,32},{48,40},{56,48},{64,88... | collective-permute-start | bytes 393224 | tf_op jit(solution)/shard_map/ppermute | solution.py:39
  31.8 0.1 pad_maximum_fusion.2
  31.9 0.1 broadcast_in_dim_tile.7.sine_ref
  32.0 0.1 copy.13
  32.1 0.1 broadcast_in_dim_tile.6.cosine_ref
  32.3 0.1 copy.16.table_cosine_ref
  32.4 0.1 copy.17.table_sine_ref
  32.5 0.0 copy-start
  32.5 0.7 copy-done
  33.2 0.0 copy-start.1
  33.2 0.7 copy-done.1
  33.8 0.7 copy-done.2
  34.5 0.7 copy-done.3
  35.2 0.6 shard_map.105
  35.8 2.8 %collective-permute-start.4 = (bf16[128,512]{1,0:T(8,128)(2,1)S(1)}, bf16[128,512]{1,0:T(8,128)(2,1)S(1)}, u32[]{:S(2)}, u32[]{:S(2)}) collective-permute-start(bf16[128,512]{1,0:T(8,128)(2,1)S(1)} %collective-permute-done), channel_id=1, source_target_pairs={{0,16},{8,24},{16,0},{24,8},{32,48},{40,56},{48,32},{56,40},{64,80... | collective-permute-start | bytes 393224 | tf_op jit(solution)/shard_map/ppermute | solution.py:39
  38.5 2.8 %collective-permute-start.1 = (bf16[128,512]{1,0:T(8,128)(2,1)S(1)}, bf16[128,512]{1,0:T(8,128)(2,1)S(1)}, u32[]{:S(2)}, u32[]{:S(2)}) collective-permute-start(bf16[128,512]{1,0:T(8,128)(2,1)S(1)} %collective-permute-done), channel_id=1, source_target_pairs={{0,8},{8,16},{16,24},{24,0},{32,40},{40,48},{48,56},{56,32},{64,72... | collective-permute-start | bytes 393224 | tf_op jit(solution)/shard_map/ppermute | solution.py:39
  41.3 0.0 collective-permute-done.7
  41.3 1.2 fusion.17
  42.5 0.0 all-to-all-done
  42.5 0.0 copy-start.5
  42.5 3.2 %collective-permute-start.3 = (bf16[512,512]{1,0:T(8,128)(2,1)S(1)}, bf16[512,512]{1,0:T(8,128)(2,1)S(1)}, u32[]{:S(2)}, u32[]{:S(2)}) collective-permute-start(bf16[512,512]{1,0:T(8,128)(2,1)S(1)} %bitcast.58), channel_id=1, source_target_pairs={{0,480},{8,488},{16,496},{24,504},{32,0},{40,8},{48,16},{56,24},{6... | collective-permute-start | bytes 1572872 | tf_op jit(solution)/shard_map/ppermute | solution.py:20
  45.7 2.9 %collective-permute-start.2 = (bf16[512,512]{1,0:T(8,128)(2,1)S(1)}, bf16[512,512]{1,0:T(8,128)(2,1)S(1)}, u32[]{:S(2)}, u32[]{:S(2)}) collective-permute-start(bf16[512,512]{1,0:T(8,128)(2,1)S(1)} %bitcast.59), channel_id=1, source_target_pairs={{0,32},{8,40},{16,48},{24,56},{32,64},{40,72},{48,80},{56,88},{64,... | collective-permute-start | bytes 1572872 | tf_op jit(solution)/shard_map/ppermute | solution.py:20
  48.7 1.5 %fusion.15 = f32[512,512]{1,0:T(8,128)S(1)} fusion(bf16[512,512]{1,0:T(8,128)(2,1)S(1)} %bitcast.60, bf16[512,4096]{1,0:T(8,128)(2,1)} %bitcast.48, u32[]{:T(128)S(6)} %mul.106), kind=kOutput, calls=%fused_computation.20 | convolution fusion | flops 268435456 | bytes 2097156 | tf_op jit(solution)/shard_map/dot_general | solution.py:60
  50.1 1.2 convolution_add_fusion.4
  51.3 6.7 %collective-permute-done.3 = bf16[512,512]{1,0:T(8,128)(2,1)S(1)} collective-permute-done((bf16[512,512]{1,0:T(8,128)(2,1)S(1)}, bf16[512,512]{1,0:T(8,128)(2,1)S(1)}, u32[]{:S(2)}, u32[]{:S(2)}) %collective-permute-start.3) | collective-permute-done | bytes 524320 | tf_op jit(solution)/shard_map/ppermute | solution.py:20
  58.0 5.6 %collective-permute-start.6 = (bf16[512,512]{1,0:T(8,128)(2,1)S(1)}, bf16[512,512]{1,0:T(8,128)(2,1)S(1)}, u32[]{:S(2)}, u32[]{:S(2)}) collective-permute-start(bf16[512,512]{1,0:T(8,128)(2,1)S(1)} %collective-permute-done.3), channel_id=1, source_target_pairs={{0,480},{8,488},{16,496},{24,504},{32,0},{40,8},{48,16},{56,24},{6... | collective-permute-start | bytes 1572872 | tf_op jit(solution)/shard_map/ppermute | solution.py:20
  63.6 0.0 collective-permute-done.2
  63.6 1.9 %collective-permute-start.5 = (bf16[512,512]{1,0:T(8,128)(2,1)S(1)}, bf16[512,512]{1,0:T(8,128)(2,1)S(1)}, u32[]{:S(2)}, u32[]{:S(2)}) collective-permute-start(bf16[512,512]{1,0:T(8,128)(2,1)S(1)} %collective-permute-done.2), channel_id=1, source_target_pairs={{0,32},{8,40},{16,48},{24,56},{32,64},{40,72},{48,80},{56,88},{64,... | collective-permute-start | bytes 1572872 | tf_op jit(solution)/shard_map/ppermute | solution.py:20
  65.5 0.0 copy-done.5
  65.5 0.4 fusion.11
  66.0 0.4 fusion.13
  66.4 8.6 %collective-permute-done.6 = bf16[512,512]{1,0:T(8,128)(2,1)S(1)} collective-permute-done((bf16[512,512]{1,0:T(8,128)(2,1)S(1)}, bf16[512,512]{1,0:T(8,128)(2,1)S(1)}, u32[]{:S(2)}, u32[]{:S(2)}) %collective-permute-start.6) | collective-permute-done | bytes 524320 | tf_op jit(solution)/shard_map/ppermute | solution.py:20
  75.0 5.6 %collective-permute-start.9 = (bf16[512,512]{1,0:T(8,128)(2,1)S(1)}, bf16[512,512]{1,0:T(8,128)(2,1)S(1)}, u32[]{:S(2)}, u32[]{:S(2)}) collective-permute-start(bf16[512,512]{1,0:T(8,128)(2,1)S(1)} %collective-permute-done.6), channel_id=1, source_target_pairs={{0,480},{8,488},{16,496},{24,504},{32,0},{40,8},{48,16},{56,24},{6... | collective-permute-start | bytes 1572872 | tf_op jit(solution)/shard_map/ppermute | solution.py:20
  80.6 0.4 fusion.7
  81.0 0.0 collective-permute-done.5
  81.0 1.9 %collective-permute-start.8 = (bf16[512,512]{1,0:T(8,128)(2,1)S(1)}, bf16[512,512]{1,0:T(8,128)(2,1)S(1)}, u32[]{:S(2)}, u32[]{:S(2)}) collective-permute-start(bf16[512,512]{1,0:T(8,128)(2,1)S(1)} %collective-permute-done.5), channel_id=1, source_target_pairs={{0,32},{8,40},{16,48},{24,56},{32,64},{40,72},{48,80},{56,88},{64,... | collective-permute-start | bytes 1572872 | tf_op jit(solution)/shard_map/ppermute | solution.py:20
  83.0 0.4 fusion.9
  83.4 0.0 collective-permute-done.4
  83.4 0.3 fusion.4
  83.7 0.0 collective-permute-done.1
  83.7 0.3 fusion.3
  84.0 12.9 %collective-permute-done.8 = bf16[512,512]{1,0:T(8,128)(2,1)S(1)} collective-permute-done((bf16[512,512]{1,0:T(8,128)(2,1)S(1)}, bf16[512,512]{1,0:T(8,128)(2,1)S(1)}, u32[]{:S(2)}, u32[]{:S(2)}) %collective-permute-start.8) | collective-permute-done | bytes 524320 | tf_op jit(solution)/shard_map/ppermute | solution.py:20
  96.9 0.4 convolution_add_fusion.1
  97.3 0.0 copy-start.4
  97.4 0.0 collective-permute-done.9
  97.4 0.4 fusion.sums_ref
  97.8 0.7 shard_map.106
  98.5 18.9 %all_to_all.15 = bf16[32,8,384]{2,1,0:T(8,128)(2,1)S(1)} all-to-all(bf16[32,8,384]{2,1,0:T(8,128)(2,1)S(1)} %bitcast.42), channel_id=1, replica_groups=mesh['gr'=2,'sp'=32,'tp'=8] {'sp'}, dimensions={0} | all-to-all | bytes 393216 | tf_op jit(solution)/shard_map/all_to_all | solution.py:351
  117.4 0.5 shard_map.107
  117.9 20.8 %all_to_all.16 = bf16[32,8,384]{2,1,0:T(8,128)(2,1)S(1)} all-to-all(bf16[32,8,384]{2,1,0:T(8,128)(2,1)S(1)} %bitcast.44), channel_id=1, replica_groups=mesh['gr'=2,'sp'=32,'tp'=8] {'sp'}, dimensions={0} | all-to-all | bytes 393216 | tf_op jit(solution)/shard_map/all_to_all | solution.py:351
  138.7 0.0 copy-done.4
  138.7 1.1 shard_map.108
  (14 shorter events, 0.1 us)
Async XLA Ops:
  2.4 40.1 %all-to-all-start = ((bf16[4,128,512]{2,1,0:T(8,128)(2,1)}), bf16[4,128,512]{2,1,0:T(8,128)(2,1)S(1)}, u32[]{:S(2)}, u32[]{:S(2)}) async-start(bf16[4,128,512]{2,1,0:T(8,128)(2,1)} %get-tuple-element.16), calls=%async_computation | async-start | bytes 1048576 | tf_op jit(solution)/shard_map/all_to_all | solution.py:44
  6.9 19.8 %collective-permute-start = (bf16[128,512]{1,0:T(8,128)(2,1)}, bf16[128,512]{1,0:T(8,128)(2,1)S(1)}, u32[]{:S(2)}, u32[]{:S(2)}) collective-permute-start(bf16[128,512]{1,0:T(8,128)(2,1)} %get-tuple-element.17), channel_id=1, source_target_pairs={{0,384},{1,129},{2,386},{3,131},{4,388},{5,133},{6,390},{7,135},{8... | collective-permute-start | bytes 393224 | tf_op jit(solution)/shard_map/ppermute | solution.py:33
  26.6 14.7 %collective-permute-start.7 = (bf16[128,512]{1,0:T(8,128)(2,1)S(1)}, bf16[128,512]{1,0:T(8,128)(2,1)S(1)}, u32[]{:S(2)}, u32[]{:S(2)}) collective-permute-start(bf16[128,512]{1,0:T(8,128)(2,1)S(1)} %collective-permute-done), channel_id=1, source_target_pairs={{0,24},{8,0},{16,8},{24,16},{32,56},{40,32},{48,40},{56,48},{64,88... | collective-permute-start | bytes 393224 | tf_op jit(solution)/shard_map/ppermute | solution.py:39
  32.5 0.7 copy-start
  33.2 0.7 copy-start.1
  33.8 0.7 copy-start.2
  34.5 0.7 copy-start.3
  35.8 47.6 %collective-permute-start.4 = (bf16[128,512]{1,0:T(8,128)(2,1)S(1)}, bf16[128,512]{1,0:T(8,128)(2,1)S(1)}, u32[]{:S(2)}, u32[]{:S(2)}) collective-permute-start(bf16[128,512]{1,0:T(8,128)(2,1)S(1)} %collective-permute-done), channel_id=1, source_target_pairs={{0,16},{8,24},{16,0},{24,8},{32,48},{40,56},{48,32},{56,40},{64,80... | collective-permute-start | bytes 393224 | tf_op jit(solution)/shard_map/ppermute | solution.py:39
  38.5 45.2 %collective-permute-start.1 = (bf16[128,512]{1,0:T(8,128)(2,1)S(1)}, bf16[128,512]{1,0:T(8,128)(2,1)S(1)}, u32[]{:S(2)}, u32[]{:S(2)}) collective-permute-start(bf16[128,512]{1,0:T(8,128)(2,1)S(1)} %collective-permute-done), channel_id=1, source_target_pairs={{0,8},{8,16},{16,24},{24,0},{32,40},{40,48},{48,56},{56,32},{64,72... | collective-permute-start | bytes 393224 | tf_op jit(solution)/shard_map/ppermute | solution.py:39
  42.5 23.0 %copy-start.5 = (bf16[4,128,4096]{2,1,0:T(8,128)(2,1)S(1)}, bf16[4,128,4096]{2,1,0:T(8,128)(2,1)}, u32[]{:S(2)}) copy-start(bf16[4,128,4096]{2,1,0:T(8,128)(2,1)} %param.9) | copy-start | bytes 12582916
  42.5 15.5 %collective-permute-start.3 = (bf16[512,512]{1,0:T(8,128)(2,1)S(1)}, bf16[512,512]{1,0:T(8,128)(2,1)S(1)}, u32[]{:S(2)}, u32[]{:S(2)}) collective-permute-start(bf16[512,512]{1,0:T(8,128)(2,1)S(1)} %bitcast.58), channel_id=1, source_target_pairs={{0,480},{8,488},{16,496},{24,504},{32,0},{40,8},{48,16},{56,24},{6... | collective-permute-start | bytes 1572872 | tf_op jit(solution)/shard_map/ppermute | solution.py:20
  45.7 17.9 %collective-permute-start.2 = (bf16[512,512]{1,0:T(8,128)(2,1)S(1)}, bf16[512,512]{1,0:T(8,128)(2,1)S(1)}, u32[]{:S(2)}, u32[]{:S(2)}) collective-permute-start(bf16[512,512]{1,0:T(8,128)(2,1)S(1)} %bitcast.59), channel_id=1, source_target_pairs={{0,32},{8,40},{16,48},{24,56},{32,64},{40,72},{48,80},{56,88},{64,... | collective-permute-start | bytes 1572872 | tf_op jit(solution)/shard_map/ppermute | solution.py:20
  58.0 17.0 %collective-permute-start.6 = (bf16[512,512]{1,0:T(8,128)(2,1)S(1)}, bf16[512,512]{1,0:T(8,128)(2,1)S(1)}, u32[]{:S(2)}, u32[]{:S(2)}) collective-permute-start(bf16[512,512]{1,0:T(8,128)(2,1)S(1)} %collective-permute-done.3), channel_id=1, source_target_pairs={{0,480},{8,488},{16,496},{24,504},{32,0},{40,8},{48,16},{56,24},{6... | collective-permute-start | bytes 1572872 | tf_op jit(solution)/shard_map/ppermute | solution.py:20
  63.6 17.4 %collective-permute-start.5 = (bf16[512,512]{1,0:T(8,128)(2,1)S(1)}, bf16[512,512]{1,0:T(8,128)(2,1)S(1)}, u32[]{:S(2)}, u32[]{:S(2)}) collective-permute-start(bf16[512,512]{1,0:T(8,128)(2,1)S(1)} %collective-permute-done.2), channel_id=1, source_target_pairs={{0,32},{8,40},{16,48},{24,56},{32,64},{40,72},{48,80},{56,88},{64,... | collective-permute-start | bytes 1572872 | tf_op jit(solution)/shard_map/ppermute | solution.py:20
  75.0 22.4 %collective-permute-start.9 = (bf16[512,512]{1,0:T(8,128)(2,1)S(1)}, bf16[512,512]{1,0:T(8,128)(2,1)S(1)}, u32[]{:S(2)}, u32[]{:S(2)}) collective-permute-start(bf16[512,512]{1,0:T(8,128)(2,1)S(1)} %collective-permute-done.6), channel_id=1, source_target_pairs={{0,480},{8,488},{16,496},{24,504},{32,0},{40,8},{48,16},{56,24},{6... | collective-permute-start | bytes 1572872 | tf_op jit(solution)/shard_map/ppermute | solution.py:20
  81.0 15.9 %collective-permute-start.8 = (bf16[512,512]{1,0:T(8,128)(2,1)S(1)}, bf16[512,512]{1,0:T(8,128)(2,1)S(1)}, u32[]{:S(2)}, u32[]{:S(2)}) collective-permute-start(bf16[512,512]{1,0:T(8,128)(2,1)S(1)} %collective-permute-done.5), channel_id=1, source_target_pairs={{0,32},{8,40},{16,48},{24,56},{32,64},{40,72},{48,80},{56,88},{64,... | collective-permute-start | bytes 1572872 | tf_op jit(solution)/shard_map/ppermute | solution.py:20
  97.3 41.3 %copy-start.4 = (f32[256]{0:T(256)S(1)}, f32[256]{0:T(256)}, u32[]{:S(2)}) copy-start(f32[256]{0:T(256)} %param.17) | copy-start | bytes 3076
